TPU v7x, 256 devices: a whole 4x4x8 slice. The times are simulated.
256 devices in a mesh: sp: 64 (over z, x, core), tp: 4 (over y).
Axes of the slice: x: 4, y: 4, z: 8, core: 2. Of those that a mesh axis runs over, the one named last changes fastest.
Arguments:
- tokens: bfloat16 [24576, 2048], P('sp', 'tp'), may hold values from -6 to 6
- norm_gain: float32 [2048], replicated, may hold values from 0.1 to 1.9
- w_pool_in: bfloat16 [2048, 2048], P('sp', 'tp'), may hold values from -0.125 to 0.125
- w_lru_in: bfloat16 [2048, 2048], P('sp', 'tp'), may hold values from -0.125 to 0.125
- pool_mix: bfloat16 [4, 512, 512], P('tp'), may hold values from -0.25 to 0.25
- conv_taps: bfloat16 [4, 2048], P(None, 'tp'), may hold values from -3 to 3
- rec_gate: bfloat16 [2, 16, 128, 128], P(None, 'tp'), may hold values from -0.5 to 0.5
- in_gate: bfloat16 [2, 16, 128, 128], P(None, 'tp'), may hold values from -0.5 to 0.5
- decay_rate: float32 [2, 2048], P(None, 'tp'), may hold values from 0 to 1, as said below
- log_decay: float32 [2, 24576], P(None, 'sp'), may hold values from -2 to 0, as said below
- start_state: float32 [2, 2048], P(None, 'tp'), may hold values from -8 to 8
- w_out_pool: bfloat16 [2048, 2048], P('tp', 'sp'), may hold values from -0.09375 to 0.09375
- w_out_lru: bfloat16 [2048, 2048], P('tp', 'sp'), may hold values from -0.09375 to 0.09375
Outputs:
- mixed: bfloat16 [24576, 2048], P(('sp', 'tp'))
Inputs may be any that keep to these rules, and one draw needn't show every extreme that they name: `decay_rate`: positive. `log_decay`: at most zero.
All inputs are finite; a program needn't handle non-finite values.
Results may differ from a plain program's by a relative error of at most 0.0068.
Values may be sent and summed in bfloat16 or wider, within the bound.
A program may use at most 64 MiB of HBM per device.

v0:
```python
import jax
import jax.numpy as jnp
from jax import lax
from jax.sharding import Mesh
from jax.sharding import PartitionSpec as P

POOL_GROUPS = 4
GRID_W = 32
SP = ("sp_0", "sp_1", "sp_2")
SP_TP = ("sp_0", "sp_1", "sp_2", "tp")


epsilon = 1e-06


def copy_for_each(array, axis):
    count = lax.axis_size(axis)
    return lax.all_to_all(
        jnp.broadcast_to(array[None], (count, *array.shape)), axis, 0, 0, tiled=True
    )


def joined_along(tiles, dim):
    tiles = jnp.moveaxis(tiles, 0, dim)
    dims = tiles.shape
    return tiles.reshape(*dims[:dim], dims[dim] * dims[dim + 1], *dims[dim + 2 :])


def gather_directly(array, axis, dim):
    tiles = copy_for_each(array, axis)
    return joined_along(tiles, dim)


def sent_together(arrays, axis, dim, along):
    both = jnp.concatenate(arrays, axis=along)
    filled, at, outs = (lax.all_gather(both, axis, axis=dim, tiled=True), 0, [])
    for a in arrays:
        outs.append(lax.slice_in_dim(filled, at, at + a.shape[along], axis=along))
        at += a.shape[along]
    return tuple(outs)


def with_halo(cells, sides, width):
    for axis, dim in sides:
        count = lax.axis_size(axis)
        ends = count - 1
        head = lax.slice_in_dim(cells, 0, width, axis=dim)
        tail = lax.slice_in_dim(cells, cells.shape[dim] - width, cells.shape[dim], axis=dim)
        cells = jnp.concatenate(
            [
                lax.ppermute(tail, axis, [(i, (i + 1) % count) for i in range(ends)]),
                cells,
                lax.ppermute(head, axis, [((i + 1) % count, i) for i in range(ends)]),
            ],
            axis=dim,
        )
    return cells


def neutral_like(array, identity):
    return jax.tree.map(
        lambda a, e: jnp.broadcast_to(jnp.asarray(e, a.dtype), a.shape), array, identity
    )


def collected_together(array, axis):
    leaves = jax.tree.leaves(array)
    sequence = sorted(range(len(leaves)), key=lambda k: -leaves[k].size)
    width = (1, *leaves[sequence[0]].shape)[-1]
    lines = [
        jnp.pad(leaves[k].reshape(-1), (0, -leaves[k].size % width)).reshape(-1, width)
        for k in sequence
    ]
    both, at, found = (lax.all_gather(jnp.concatenate(lines), axis), 0, {})
    for k, line in zip(sequence, lines):
        slab = both[:, at : at + len(line)].reshape(len(both), -1)
        found[k] = slab[:, : leaves[k].size].reshape(-1, *leaves[k].shape)
        at += len(line)
    numbers = iter(range(len(leaves)))
    return jax.tree.map(lambda _: found[next(numbers)], array)


def prefix_by_axis(array, axes, combine, identity):
    before = start = neutral_like(array, identity)
    running = array
    for axis in reversed(axes):
        count, mine = (lax.axis_size(axis), lax.axis_index(axis))
        pieces = collected_together(running, axis)
        inside, running = (start, start)
        for k in range(count):
            passed = k < mine
            running = combine(running, jax.tree.map(lambda part: part[k], pieces))
            inside = jax.tree.map(lambda new, old: jnp.where(passed, new, old), running, inside)
        before = combine(inside, before)
    return before


def gathered_once(array, axis):
    leaves = jax.tree.leaves(array)
    sequence = sorted(range(len(leaves)), key=lambda k: -leaves[k].size)
    width = (1, *leaves[sequence[0]].shape)[-1]
    lines = [
        jnp.pad(leaves[k].reshape(-1), (0, -leaves[k].size % width)).reshape(-1, width)
        for k in sequence
    ]
    both, at, found = (copy_for_each(jnp.concatenate(lines), axis), 0, {})
    for k, line in zip(sequence, lines):
        slab = both[:, at : at + len(line)].reshape(len(both), -1)
        found[k] = slab[:, : leaves[k].size].reshape(-1, *leaves[k].shape)
        at += len(line)
    numbers = iter(range(len(leaves)))
    return jax.tree.map(lambda _: found[next(numbers)], array)


def folded_in_pairs(pieces, combine):
    while len(jax.tree.leaves(pieces)[0]) > 1:
        pieces = jax.vmap(combine)(
            *(jax.tree.map(lambda part: part[side::2], pieces) for side in (0, 1))
        )
    return jax.tree.map(lambda part: part[0], pieces)


def entering(array, axis, combine, identity):
    count, mine = (lax.axis_size(axis), lax.axis_index(axis))
    passed = jnp.arange(count) > mine

    def kept(part, zero, own):
        part = jnp.where(
            passed.reshape(-1, *(1 for _ in own.shape)), part, jnp.asarray(zero, own.dtype)
        )
        return part[::-1]

    pieces = gathered_once(array, axis)
    return folded_in_pairs(jax.tree.map(kept, pieces, identity, array), combine)


def rows_first(arrays, axis, dims):
    turned = [jnp.moveaxis(a, dim, 0) for a, dim in zip(arrays, dims)]
    widths = [t[0].size for t in turned]
    both = jnp.concatenate([t.reshape(-1, w) for t, w in zip(turned, widths)], axis=1)
    filled = lax.all_gather(both, axis, axis=0, tiled=True)
    tiles = jnp.split(filled, [sum(widths[:k]) for k in range(1, len(widths))], axis=1)
    return tuple(
        (
            jnp.moveaxis(b.reshape(-1, *t.shape[1:]), 0, dim)
            for b, t, dim in zip(tiles, turned, dims)
        )
    )


def in_blocks(array, dim, count):
    before, after = (array.shape[:dim], array.shape[dim + 1 :])
    return jnp.moveaxis(array.reshape(*before, count, -1, *after), dim, 0)


def sent_and_summed(array, axis, dim):
    count = lax.axis_size(axis)
    tiles = lax.all_to_all(in_blocks(array, dim, count), axis, 0, 0, tiled=True)
    return jnp.sum(tiles.astype(jnp.float32), axis=0)


def link_pair(earlier, later_pair):
    return (earlier[0] * later_pair[0], later_pair[0] * earlier[1] + later_pair[1])


def per_device(
    tokens,
    norm_gain,
    w_pool_in,
    w_lru_in,
    pool_mix,
    conv_taps,
    rec_gate,
    in_gate,
    decay_rate,
    log_decay,
    start_state,
    w_out_pool,
    w_out_lru,
):
    tok_rows = tokens.shape[0]
    pool_width = w_pool_in.shape[1]
    lru_width = w_lru_in.shape[1]
    whole_rows = gather_directly(tokens, "tp", 1)
    values = whole_rows.astype(jnp.float32)
    root_mean_square_scale = lax.rsqrt(jnp.mean(values * values, axis=1, keepdims=True) + epsilon)
    normed = (values * root_mean_square_scale * norm_gain).astype(jnp.bfloat16)
    pieces = sent_together((w_pool_in, w_lru_in), SP, 0, 1)
    sum_pool = jnp.dot(normed, pieces[0], preferred_element_type=jnp.float32)
    sum_lru = jnp.dot(normed, pieces[1], preferred_element_type=jnp.float32)
    u_pool = sum_pool.astype(jnp.bfloat16)
    u_lru = sum_lru.astype(jnp.bfloat16)
    grid_rows = tok_rows // GRID_W
    reach = 2 ** (POOL_GROUPS - 1)
    grid_pooled_image = u_pool.reshape(grid_rows, GRID_W, pool_width)
    extended = with_halo(grid_pooled_image, ((SP, 0),), reach)
    half_span = jnp.left_shift(jnp.int32(1), lax.axis_index("tp"))
    row_count = grid_rows * lax.axis_size(SP)
    first_row = lax.axis_index(SP) * grid_rows
    local_rows = first_row + jnp.arange(grid_rows, dtype=jnp.int32)
    row_lower = jnp.clip(local_rows - half_span, 0, row_count)
    row_upper = jnp.clip(local_rows + half_span, 0, row_count)
    halo_rows = first_row - reach + jnp.arange(grid_rows + 2 * reach, dtype=jnp.int32)
    row_box = (
        (halo_rows[None, :] >= row_lower[:, None]) & (halo_rows[None, :] < row_upper[:, None])
    ).astype(jnp.bfloat16)
    col_index = jnp.arange(GRID_W, dtype=jnp.int32)
    col_lower = jnp.clip(col_index - half_span, 0, GRID_W)
    col_upper = jnp.clip(col_index + half_span, 0, GRID_W)
    col_box = (
        (col_index[None, :] >= col_lower[:, None]) & (col_index[None, :] < col_upper[:, None])
    ).astype(jnp.float32)
    row_sums = jnp.einsum("ae,ecz->acz", row_box, extended, preferred_element_type=jnp.float32)
    box_total = jnp.einsum("bc,acz->abz", col_box, row_sums, precision=lax.Precision.HIGHEST)
    counts = ((row_upper - row_lower)[:, None] * (col_upper - col_lower)[None, :]).astype(
        jnp.float32
    )
    pool_diff = (box_total / counts[:, :, None] - grid_pooled_image.astype(jnp.float32)).astype(
        jnp.bfloat16
    )
    y_pool = jnp.dot(
        pool_diff.reshape(tok_rows, pool_width), pool_mix[0], preferred_element_type=jnp.float32
    ).astype(jnp.bfloat16)
    tap_count = conv_taps.shape[0]
    left_taps = tap_count // 2
    padded = with_halo(u_lru, ((SP, 0),), left_taps)
    tap_weights = conv_taps.astype(jnp.float32)
    conv_sum = padded[0:tok_rows].astype(jnp.float32) * tap_weights[0]
    for tap_index in range(1, tap_count):
        conv_sum = (
            conv_sum
            + padded[tap_index : tap_index + tok_rows].astype(jnp.float32) * tap_weights[tap_index]
        )
    conv_in = conv_sum.astype(jnp.bfloat16)
    head_size = rec_gate.shape[2]
    blocks = conv_in.reshape(tok_rows, lru_width // head_size, head_size)
    drive_in = conv_in.astype(jnp.float32)
    local_scans = []
    for direction in range(2):
        recur_gate = jax.nn.sigmoid(
            jnp.einsum(
                "tnc,ncd->tnd", blocks, rec_gate[direction], preferred_element_type=jnp.float32
            ).reshape(tok_rows, lru_width)
        )
        input_gate = jax.nn.sigmoid(
            jnp.einsum(
                "tnc,ncd->tnd", blocks, in_gate[direction], preferred_element_type=jnp.float32
            ).reshape(tok_rows, lru_width)
        )
        log_keep = -8.0 * recur_gate * decay_rate[direction] + log_decay[direction][:, None]
        keep_rate = jnp.exp(log_keep)
        drive_term = jnp.sqrt(-jnp.expm1(2.0 * log_keep)) * input_gate * drive_in
        local_scans.append(
            lax.associative_scan(link_pair, (keep_rate, drive_term), reverse=direction == 1, axis=0)
        )
    forward_prod, leftward_running_total = local_scans[0]
    reverse_decay_product, backward_sum = local_scans[1]
    unit_rate = jnp.ones((lru_width,), jnp.float32)
    nothing = jnp.zeros((lru_width,), jnp.float32)
    enter_forward = prefix_by_axis(
        (forward_prod[-1], leftward_running_total[-1]), SP, link_pair, (unit_rate, nothing)
    )
    enter_backward = entering(
        (reverse_decay_product[0], backward_sum[0]), SP, link_pair, (unit_rate, nothing)
    )
    state_forward = enter_forward[0] * start_state[0] + enter_forward[1]
    state_backward = enter_backward[0] * start_state[1] + enter_backward[1]
    y_lru = (
        forward_prod * state_forward
        + leftward_running_total
        + reverse_decay_product * state_backward
        + backward_sum
    ).astype(jnp.bfloat16)
    weight_pool, weight_lru = rows_first((w_out_pool, w_out_lru), SP, (1, 1))
    mixed = sent_and_summed(
        (
            jnp.dot(y_pool, weight_pool, preferred_element_type=jnp.float32)
            + jnp.dot(y_lru, weight_lru, preferred_element_type=jnp.float32)
        ).astype(jnp.bfloat16),
        "tp",
        0,
    )
    return mixed.astype(jnp.bfloat16)


def solution(mesh):
    torus = Mesh(mesh.devices.reshape(8, 4, 2, mesh.shape["tp"]), ("sp_0", "sp_1", "sp_2", "tp"))
    in_specs = (
        P(SP, "tp"),
        P(),
        P(SP, "tp"),
        P(SP, "tp"),
        P("tp", None, None),
        P(None, "tp"),
        P(None, "tp", None, None),
        P(None, "tp", None, None),
        P(None, "tp"),
        P(None, SP),
        P(None, "tp"),
        P("tp", SP),
        P("tp", SP),
    )
    out_specs = P(SP_TP, None)
    return jax.shard_map(
        per_device, mesh=torus, in_specs=in_specs, out_specs=out_specs, check_vma=False
    )
```

profile of v0, /device:TPU:8, one launch (start us, length us, event | category | flops | bytes accessed | tf_op | source)
XLA Modules:
  0.0 336.0 jit_solution(10510905345906210611)
XLA Ops:
  6.5 1.5 pad_maximum_fusion.14
  8.0 1.2 copy.39
  9.3 1.3 broadcast_in_dim.22
  10.6 5.8 %all-to-all-start = ((bf16[4,384,512]{1,2,0:T(8,128)(2,1)}), bf16[4,384,512]{1,2,0:T(8,128)(2,1)S(1)}, u32[]{:S(2)}, u32[]{:S(2)}) async-start(bf16[4,384,512]{1,2,0:T(8,128)(2,1)} %broadcast_in_dim.22), calls=%async_computation | async-start | bytes 3145728 | tf_op jit(solution)/shard_map/all_to_all | solution.py:18
  20.0 14.9 %all-to-all-done = bf16[4,384,512]{1,2,0:T(8,128)(2,1)S(1)} async-done(((bf16[4,384,512]{1,2,0:T(8,128)(2,1)}), bf16[4,384,512]{1,2,0:T(8,128)(2,1)S(1)}, u32[]{:S(2)}, u32[]{:S(2)}) %all-to-all-start) | async-done | bytes 1572896 | tf_op jit(solution)/shard_map/all_to_all | solution.py:18
  35.3 1.6 fusion.1
  36.9 55.2 %all-gather.9.cloned.1.call-done = bf16[2048,1024]{1,0:T(8,128)(2,1)} async-done(((bf16[32,1024]{1,0:T(8,128)(2,1)}), bf16[2048,1024]{1,0:T(8,128)(2,1)}) %all-gather.9.cloned.1.call-update) | async-done | bytes 4194320 | tf_op jit(solution)/shard_map/all_gather | solution.py:36
  92.0 3.1 fusion.27
  95.1 1.3 collective-permute-start.3
  96.4 3.0 collective-permute-start.2
  99.5 2.6 fusion.24
  102.1 1.0 copy.42
  104.0 0.9 copy.41
  104.8 1.3 collective-permute-start.1
  106.1 4.7 %collective-permute-start = (bf16[8,32,512]{2,0,1:T(8,128)(2,1)}, bf16[8,32,512]{2,0,1:T(8,128)(2,1)}, u32[]{:S(2)}, u32[]{:S(2)}) collective-permute-start(bf16[8,32,512]{2,0,1:T(8,128)(2,1)} %copy.40), channel_id=1, source_target_pairs={{0,4},{4,8},{8,12},{12,16},{16,20},{20,24},{24,28},{28,32},{32,36}... | collective-permute-start | bytes 786440 | tf_op jit(solution)/shard_map/ppermute | solution.py:51
  112.6 1.4 fusion.16
  114.4 1.2 copy.58
  115.6 2.3 copy.59
  117.8 1.2 copy.60
  119.1 1.2 copy.57
  120.3 3.2 fusion.37
  123.6 0.9 copy-done.1
  125.0 3.2 slice.879
  128.2 3.1 slice.844
  131.4 3.2 slice.843
  135.1 1.5 slice.919
  136.6 1.4 slice.884
  138.0 1.5 slice.883
  139.5 1.5 fusion.127
  145.0 1.0 fusion.132
  161.4 1.4 slice.1035
  163.3 1.4 slice.997
  165.3 1.4 slice.992
  167.2 1.5 slice.954
  170.2 3.5 %slice.955 = f32[192,512]{1,0:T(8,128)S(1)} reverse(f32[192,512]{1,0:T(8,128)} %slice.954), dimensions={0} | reverse | bytes 786432 | tf_op jit(solution)/shard_map/slice | solution.py:254
  173.7 2.7 slice.957
  176.3 1.1 fusion.128
  197.2 1.1 pad.209
  198.3 1.0 pad.225
  200.9 1.0 add_multiply_fusion.3
  202.0 1.9 pad.226
  204.6 1.9 pad.210
  206.7 1.9 pad.211
  208.6 1.9 pad.227
  210.5 0.9 slice.1036
  211.4 0.9 slice.993
  215.5 1.0 pad.241
  218.2 1.0 add_multiply_fusion.1
  220.3 1.2 pad.243
  221.5 1.0 add.750
  222.5 6.9 %rev.4 = f32[384,512]{1,0:T(8,128)} reverse(f32[384,512]{1,0:T(8,128)} %add.750), dimensions={0} | reverse | bytes 1572864 | tf_op jit(solution)/shard_map/rev | solution.py:254
  229.3 2.9 pad.259
  232.2 2.2 add.776
  234.4 6.8 %rev.5 = f32[384,512]{1,0:T(8,128)} reverse(f32[384,512]{1,0:T(8,128)} %add.776), dimensions={0} | reverse | bytes 1572864 | tf_op jit(solution)/shard_map/rev | solution.py:254
  242.7 13.4 %all-to-all-start.1 = ((f32[64,2,512]{2,1,0:T(2,128)}), f32[64,2,512]{2,1,0:T(2,128)S(1)}, u32[]{:S(2)}, u32[]{:S(2)}) async-start(f32[64,2,512]{2,1,0:T(2,128)} %broadcast_in_dim.26), calls=%async_computation.1 | async-start | bytes 524288 | tf_op jit(solution)/shard_map/all_to_all | solution.py:18
  257.6 1.8 all-gather.3
  259.4 12.5 %all-gather.4 = f32[4,2,512]{2,1,0:T(2,128)S(1)} all-gather(f32[1,2,512]{2,1,0:T(2,128)S(1)} %maximum_bitcast_fusion.1), channel_id=3, replica_groups=mesh['sp_0'=8,'sp_1'=4,'sp_2'=2,'tp'=4] {'sp_1'}, dimensions={0}, use_global_device_ids=true | all-gather | bytes 20480 | tf_op jit(solution)/shard_map/all_gather | solution.py:74
  272.0 26.0 %all-gather.5 = f32[8,2,512]{2,1,0:T(2,128)S(1)} all-gather(f32[1,2,512]{2,1,0:T(2,128)S(1)} %maximum_bitcast_fusion.2), channel_id=4, replica_groups=mesh['sp_0'=8,'sp_1'=4,'sp_2'=2,'tp'=4] {'sp_0'}, dimensions={0}, use_global_device_ids=true | all-gather | bytes 36864 | tf_op jit(solution)/shard_map/all_gather | solution.py:74
  298.0 1.5 fusion.30
  299.6 1.1 fusion.23
  300.7 4.5 %fusion.5 = f32[384,2048]{1,0:T(8,128)} fusion(bf16[2048,1024]{1,0:T(8,128)(2,1)} %all-gather.11.cloned.1.call-done, bf16[384,512]{1,0:T(8,128)(2,1)S(1)} %bitcast.293, bf16[1,512,512]{2,1,0:T(8,128)(2,1)S(1)} %copy-done), kind=kOutput, calls=%fused_computation.8 | convolution fusion | flops 1006829568 | bytes 6160384 | tf_op jit(solution)/shard_map/dot_general | solution.py:277
  306.9 4.4 %add_convert_fusion = bf16[384,2048]{1,0:T(8,128)(2,1)S(1)} fusion(f32[384,2048]{1,0:T(8,128)} %fusion.5, bf16[2048,1024]{1,0:T(8,128)(2,1)} %all-gather.11.cloned.1.call-done, f32[384,512]{1,0:T(8,128)} %rev.5, f32[384,512]{1,0:T(8,128)} %rev.4, f32[384,512]{1,0:T(8,128)S(1)} %copy-done.2, f32[384,512]{1,0:T(8,128)} %pad.227, f32[384,512]{1,0:T(8,128)S(1)} %copy-done.3, ...), kind=kOutput, calls=%fused_computation.3 | convolution fusion | flops 808452096 | bytes 11538432 | tf_op jit(solution)/shard_map/dot_general | solution.py:278
  311.3 16.8 %all_to_all.15 = bf16[4,96,2048]{2,1,0:T(8,128)(2,1)S(1)} all-to-all(bf16[4,96,2048]{2,1,0:T(8,128)(2,1)S(1)} %bitcast.284), channel_id=1, replica_groups=mesh['sp_0'=8,'sp_1'=4,'sp_2'=2,'tp'=4] {'tp'}, dimensions={0} | all-to-all | bytes 3145728 | tf_op jit(solution)/shard_map/all_to_all | solution.py:158
  328.1 1.1 reduce_sum.22
  (484 shorter events, 61.8 us)
Async XLA Ops:
  6.5 294.2 %copy-start = (bf16[1,512,512]{2,1,0:T(8,128)(2,1)S(1)}, bf16[1,512,512]{2,1,0:T(8,128)(2,1)}, u32[]{:S(2)}) copy-start(bf16[1,512,512]{2,1,0:T(8,128)(2,1)} %param.17) | copy-start | bytes 1572868
  6.5 85.5 %all-gather.9.cloned.1.call-start = ((), (), s32[]{:S(2)}) async-start(), calls=%async_computation.3 | async-start | bytes 4259840 | tf_op jit(solution)/shard_map/all_gather | solution.py:36
  9.2 7.2 %copy-start.42 = (bf16[512,32]{0,1:T(8,128)(2,1)S(1)}, bf16[512,32]{0,1:T(8,128)(2,1)}, u32[]{:S(2)}) copy-start(bf16[512,32]{0,1:T(8,128)(2,1)} %param.25) | copy-start | bytes 98308
  9.3 7.1 %copy-start.43 = (bf16[512,32]{0,1:T(8,128)(2,1)S(1)}, bf16[512,32]{0,1:T(8,128)(2,1)}, u32[]{:S(2)}) copy-start(bf16[512,32]{0,1:T(8,128)(2,1)} %param.24) | copy-start | bytes 98308
  10.6 8.7 %copy-start.80 = (f32[2,384]{1,0:T(2,128)S(1)}, f32[2,384]{1,0:T(2,128)}, u32[]{:S(2)}) copy-start(f32[2,384]{1,0:T(2,128)} %param.22) | copy-start | bytes 9220
  10.6 8.7 %copy-start.78 = (f32[2,512]{1,0:T(2,128)S(1)}, f32[2,512]{1,0:T(2,128)}, u32[]{:S(2)}) copy-start(f32[2,512]{1,0:T(2,128)} %param.21) | copy-start | bytes 12292
  10.6 9.4 %copy-start.48 = (bf16[4,512]{1,0:T(4,128)(2,1)S(1)}, bf16[4,512]{1,0:T(4,128)(2,1)}, u32[]{:S(2)}) copy-start(bf16[4,512]{1,0:T(4,128)(2,1)} %param.18) | copy-start | bytes 12292
  10.6 24.7 %copy-start.49 = (f32[2048]{0:T(1024)S(1)}, f32[2048]{0:T(1024)}, u32[]{:S(2)}) copy-start(f32[2048]{0:T(1024)} %param.14) | copy-start | bytes 24580
  10.6 24.3 %all-to-all-start = ((bf16[4,384,512]{1,2,0:T(8,128)(2,1)}), bf16[4,384,512]{1,2,0:T(8,128)(2,1)S(1)}, u32[]{:S(2)}, u32[]{:S(2)}) async-start(bf16[4,384,512]{1,2,0:T(8,128)(2,1)} %broadcast_in_dim.22), calls=%async_computation | async-start | bytes 3145728 | tf_op jit(solution)/shard_map/all_to_all | solution.py:18
  16.4 284.3 %all-gather.11.cloned.1.call-start = ((), (), s32[]{:S(2)}) async-start(), calls=%async_computation.4 | async-start | bytes 4259840 | tf_op jit(solution)/shard_map/all_gather | solution.py:141
  36.9 62.6 %copy-start.13 = (bf16[384,2048]{0,1:T(8,128)(2,1)S(1)}, bf16[384,2048]{0,1:T(8,128)(2,1)}, u32[]{:S(2)}) copy-start(bf16[384,2048]{0,1:T(8,128)(2,1)} %fusion.1) | copy-start | bytes 4718596
  95.1 15.7 %collective-permute-start.3 = (bf16[2,512]{1,0:T(2,128)(2,1)S(1)}, bf16[2,512]{1,0:T(2,128)(2,1)S(1)}, u32[]{:S(2)}, u32[]{:S(2)}) collective-permute-start(bf16[2,512]{1,0:T(2,128)(2,1)S(1)} %get-tuple-element.32), channel_id=1, source_target_pairs={{4,0},{8,4},{12,8},{16,12},{20,16},{24,20},{28,24},{32,28},{36,32}... | collective-permute-start | bytes 6152 | tf_op jit(solution)/shard_map/ppermute | solution.py:53
  96.4 14.4 %collective-permute-start.2 = (bf16[2,512]{1,0:T(2,128)(2,1)S(1)}, bf16[2,512]{1,0:T(2,128)(2,1)S(1)}, u32[]{:S(2)}, u32[]{:S(2)}) collective-permute-start(bf16[2,512]{1,0:T(2,128)(2,1)S(1)} %get-tuple-element.33), channel_id=1, source_target_pairs={{0,4},{4,8},{8,12},{12,16},{16,20},{20,24},{24,28},{28,32},{32,36}... | collective-permute-start | bytes 6152 | tf_op jit(solution)/shard_map/ppermute | solution.py:51
  102.1 9.1 %copy-start.82 = (bf16[2,4,128,128]{3,2,1,0:T(8,128)(2,1)S(1)}, bf16[2,4,128,128]{3,2,1,0:T(8,128)(2,1)}, u32[]{:S(2)}) copy-start(bf16[2,4,128,128]{3,2,1,0:T(8,128)(2,1)} %param.20) | copy-start | bytes 786436
  104.8 193.2 %collective-permute-start.1 = (bf16[8,32,512]{2,0,1:T(8,128)(2,1)}, bf16[8,32,512]{2,0,1:T(8,128)(2,1)}, u32[]{:S(2)}, u32[]{:S(2)}) collective-permute-start(bf16[8,32,512]{2,0,1:T(8,128)(2,1)} %copy.41), channel_id=1, source_target_pairs={{4,0},{8,4},{12,8},{16,12},{20,16},{24,20},{28,24},{32,28},{36,32}... | collective-permute-start | bytes 786440 | tf_op jit(solution)/shard_map/ppermute | solution.py:53
  106.1 191.9 %collective-permute-start = (bf16[8,32,512]{2,0,1:T(8,128)(2,1)}, bf16[8,32,512]{2,0,1:T(8,128)(2,1)}, u32[]{:S(2)}, u32[]{:S(2)}) collective-permute-start(bf16[8,32,512]{2,0,1:T(8,128)(2,1)} %copy.40), channel_id=1, source_target_pairs={{0,4},{4,8},{8,12},{12,16},{16,20},{20,24},{24,28},{28,32},{32,36}... | collective-permute-start | bytes 786440 | tf_op jit(solution)/shard_map/ppermute | solution.py:51
  164.7 3.9 %copy-start.12 = (f32[192,512]{1,0:T(8,128)S(1)}, f32[192,512]{1,0:T(8,128)}, u32[]{:S(2)}) copy-start(f32[192,512]{1,0:T(8,128)} %slice.997) | copy-start | bytes 1179652
  180.2 14.0 %copy-start.38 = (f32[3,512]{1,0:T(4,128)S(1)}, f32[3,512]{1,0:T(4,128)}, u32[]{:S(2)}) copy-start(f32[3,512]{1,0:T(4,128)} %slice.862) | copy-start | bytes 18436
  180.2 14.0 %copy-start.39 = (f32[3,512]{1,0:T(4,128)S(1)}, f32[3,512]{1,0:T(4,128)}, u32[]{:S(2)}) copy-start(f32[3,512]{1,0:T(4,128)} %slice.861) | copy-start | bytes 18436
  180.3 13.9 %copy-start.40 = (f32[3,512]{1,0:T(4,128)S(1)}, f32[3,512]{1,0:T(4,128)}, u32[]{:S(2)}) copy-start(f32[3,512]{1,0:T(4,128)} %slice.902) | copy-start | bytes 18436
  180.3 13.9 %copy-start.41 = (f32[3,512]{1,0:T(4,128)S(1)}, f32[3,512]{1,0:T(4,128)}, u32[]{:S(2)}) copy-start(f32[3,512]{1,0:T(4,128)} %slice.901) | copy-start | bytes 18436
  180.3 14.1 %copy-start.46 = (f32[2,512]{1,0:T(2,128)S(1)}, f32[2,512]{1,0:T(2,128)}, u32[]{:S(2)}) copy-start(f32[2,512]{1,0:T(2,128)} %slice.867) | copy-start | bytes 12292
  180.3 14.1 %copy-start.47 = (f32[2,512]{1,0:T(2,128)S(1)}, f32[2,512]{1,0:T(2,128)}, u32[]{:S(2)}) copy-start(f32[2,512]{1,0:T(2,128)} %slice.907) | copy-start | bytes 12292
  180.3 14.1 %copy-start.76 = (f32[1,512]{1,0:T(1,128)S(1)}, f32[1,512]{1,0:T(1,128)}, u32[]{:S(2)}) copy-start(f32[1,512]{1,0:T(1,128)} %slice.1113) | copy-start | bytes 6148
  180.3 14.1 %copy-start.75 = (f32[1,512]{1,0:T(1,128)S(1)}, f32[1,512]{1,0:T(1,128)}, u32[]{:S(2)}) copy-start(f32[1,512]{1,0:T(1,128)} %slice.1087) | copy-start | bytes 6148
  180.3 14.2 %copy-start.32 = (f32[5,512]{1,0:T(8,128)S(1)}, f32[5,512]{1,0:T(8,128)}, u32[]{:S(2)}) copy-start(f32[5,512]{1,0:T(8,128)} %slice.869) | copy-start | bytes 30724
  180.3 14.2 %copy-start.33 = (f32[5,512]{1,0:T(8,128)S(1)}, f32[5,512]{1,0:T(8,128)}, u32[]{:S(2)}) copy-start(f32[5,512]{1,0:T(8,128)} %slice.909) | copy-start | bytes 30724
  180.9 13.7 %copy-start.74 = (f32[1,512]{1,0:T(1,128)S(1)}, f32[1,512]{1,0:T(1,128)}, u32[]{:S(2)}) copy-start(f32[1,512]{1,0:T(1,128)} %slice.1112) | copy-start | bytes 6148
  181.6 13.0 %copy-start.73 = (f32[1,512]{1,0:T(1,128)S(1)}, f32[1,512]{1,0:T(1,128)}, u32[]{:S(2)}) copy-start(f32[1,512]{1,0:T(1,128)} %slice.1086) | copy-start | bytes 6148
  181.7 13.1 %copy-start.28 = (f32[11,512]{1,0:T(8,128)S(1)}, f32[11,512]{1,0:T(8,128)}, u32[]{:S(2)}) copy-start(f32[11,512]{1,0:T(8,128)} %slice.871) | copy-start | bytes 67588
  181.7 13.1 %copy-start.29 = (f32[11,512]{1,0:T(8,128)S(1)}, f32[11,512]{1,0:T(8,128)}, u32[]{:S(2)}) copy-start(f32[11,512]{1,0:T(8,128)} %slice.911) | copy-start | bytes 67588
  183.0 11.8 %copy-start.70 = (f32[1,512]{1,0:T(1,128)S(1)}, f32[1,512]{1,0:T(1,128)}, u32[]{:S(2)}) copy-start(f32[1,512]{1,0:T(1,128)} %slice.1085) | copy-start | bytes 6148
  183.0 11.8 %copy-start.69 = (f32[1,512]{1,0:T(1,128)S(1)}, f32[1,512]{1,0:T(1,128)}, u32[]{:S(2)}) copy-start(f32[1,512]{1,0:T(1,128)} %slice.1111) | copy-start | bytes 6148
  183.1 11.9 %copy-start.25 = (f32[23,512]{1,0:T(8,128)S(1)}, f32[23,512]{1,0:T(8,128)}, u32[]{:S(2)}) copy-start(f32[23,512]{1,0:T(8,128)} %slice.873) | copy-start | bytes 141316
  183.1 11.9 %copy-start.26 = (f32[23,512]{1,0:T(8,128)S(1)}, f32[23,512]{1,0:T(8,128)}, u32[]{:S(2)}) copy-start(f32[23,512]{1,0:T(8,128)} %slice.913) | copy-start | bytes 141316
  183.8 11.2 %copy-start.67 = (f32[1,512]{1,0:T(1,128)S(1)}, f32[1,512]{1,0:T(1,128)}, u32[]{:S(2)}) copy-start(f32[1,512]{1,0:T(1,128)} %slice.1110) | copy-start | bytes 6148
  185.0 10.0 %copy-start.65 = (f32[1,512]{1,0:T(1,128)S(1)}, f32[1,512]{1,0:T(1,128)}, u32[]{:S(2)}) copy-start(f32[1,512]{1,0:T(1,128)} %slice.1084) | copy-start | bytes 6148
  188.2 7.0 %copy-start.22 = (f32[47,512]{1,0:T(8,128)S(1)}, f32[47,512]{1,0:T(8,128)}, u32[]{:S(2)}) copy-start(f32[47,512]{1,0:T(8,128)} %slice.875) | copy-start | bytes 288772
  188.2 7.0 %copy-start.23 = (f32[47,512]{1,0:T(8,128)S(1)}, f32[47,512]{1,0:T(8,128)}, u32[]{:S(2)}) copy-start(f32[47,512]{1,0:T(8,128)} %slice.915) | copy-start | bytes 288772
  201.9 4.7 %copy-start.15 = (f32[192,512]{1,0:T(8,128)S(1)}, f32[192,512]{1,0:T(8,128)}, u32[]{:S(2)}) copy-start(f32[192,512]{1,0:T(8,128)} %add.692) | copy-start | bytes 1179652
  202.0 6.6 %copy-start.14 = (f32[192,512]{1,0:T(8,128)S(1)}, f32[192,512]{1,0:T(8,128)}, u32[]{:S(2)}) copy-start(f32[192,512]{1,0:T(8,128)} %add.717) | copy-start | bytes 1179652
  203.9 6.7 %copy-start.7 = (f32[191,512]{1,0:T(8,128)S(1)}, f32[191,512]{1,0:T(8,128)}, u32[]{:S(2)}) copy-start(f32[191,512]{1,0:T(8,128)} %slice.1035) | copy-start | bytes 1173508
  204.6 6.8 %copy-start.8 = (f32[191,512]{1,0:T(8,128)S(1)}, f32[191,512]{1,0:T(8,128)}, u32[]{:S(2)}) copy-start(f32[191,512]{1,0:T(8,128)} %slice.992) | copy-start | bytes 1173508
  206.6 5.7 %copy-start.34 = (f32[3,512]{1,0:T(4,128)S(1)}, f32[3,512]{1,0:T(4,128)}, u32[]{:S(2)}) copy-start(f32[3,512]{1,0:T(4,128)} %slice.975) | copy-start | bytes 18436
  206.6 5.7 %copy-start.35 = (f32[3,512]{1,0:T(4,128)S(1)}, f32[3,512]{1,0:T(4,128)}, u32[]{:S(2)}) copy-start(f32[3,512]{1,0:T(4,128)} %slice.974) | copy-start | bytes 18436
  206.6 5.7 %copy-start.36 = (f32[3,512]{1,0:T(4,128)S(1)}, f32[3,512]{1,0:T(4,128)}, u32[]{:S(2)}) copy-start(f32[3,512]{1,0:T(4,128)} %slice.1018) | copy-start | bytes 18436
  206.6 5.7 %copy-start.37 = (f32[3,512]{1,0:T(4,128)S(1)}, f32[3,512]{1,0:T(4,128)}, u32[]{:S(2)}) copy-start(f32[3,512]{1,0:T(4,128)} %slice.1017) | copy-start | bytes 18436
  206.6 5.9 %copy-start.44 = (f32[2,512]{1,0:T(2,128)S(1)}, f32[2,512]{1,0:T(2,128)}, u32[]{:S(2)}) copy-start(f32[2,512]{1,0:T(2,128)} %slice.980) | copy-start | bytes 12292
  206.6 5.9 %copy-start.45 = (f32[2,512]{1,0:T(2,128)S(1)}, f32[2,512]{1,0:T(2,128)}, u32[]{:S(2)}) copy-start(f32[2,512]{1,0:T(2,128)} %slice.1023) | copy-start | bytes 12292
  206.6 5.9 %copy-start.72 = (f32[1,512]{1,0:T(1,128)S(1)}, f32[1,512]{1,0:T(1,128)}, u32[]{:S(2)}) copy-start(f32[1,512]{1,0:T(1,128)} %slice.1193) | copy-start | bytes 6148
  206.6 5.9 %copy-start.71 = (f32[1,512]{1,0:T(1,128)S(1)}, f32[1,512]{1,0:T(1,128)}, u32[]{:S(2)}) copy-start(f32[1,512]{1,0:T(1,128)} %slice.1167) | copy-start | bytes 6148
  206.7 6.0 %copy-start.30 = (f32[5,512]{1,0:T(8,128)S(1)}, f32[5,512]{1,0:T(8,128)}, u32[]{:S(2)}) copy-start(f32[5,512]{1,0:T(8,128)} %slice.982) | copy-start | bytes 30724
  206.7 6.0 %copy-start.31 = (f32[5,512]{1,0:T(8,128)S(1)}, f32[5,512]{1,0:T(8,128)}, u32[]{:S(2)}) copy-start(f32[5,512]{1,0:T(8,128)} %slice.1025) | copy-start | bytes 30724
  206.7 6.1 %copy-start.68 = (f32[1,512]{1,0:T(1,128)S(1)}, f32[1,512]{1,0:T(1,128)}, u32[]{:S(2)}) copy-start(f32[1,512]{1,0:T(1,128)} %slice.1192) | copy-start | bytes 6148
  206.7 6.1 %copy-start.66 = (f32[1,512]{1,0:T(1,128)S(1)}, f32[1,512]{1,0:T(1,128)}, u32[]{:S(2)}) copy-start(f32[1,512]{1,0:T(1,128)} %slice.1166) | copy-start | bytes 6148
  208.6 4.3 %copy-start.27 = (f32[11,512]{1,0:T(8,128)S(1)}, f32[11,512]{1,0:T(8,128)}, u32[]{:S(2)}) copy-start(f32[11,512]{1,0:T(8,128)} %slice.1027) | copy-start | bytes 67588
  208.6 4.3 %copy-start.64 = (f32[1,512]{1,0:T(1,128)S(1)}, f32[1,512]{1,0:T(1,128)}, u32[]{:S(2)}) copy-start(f32[1,512]{1,0:T(1,128)} %slice.1165) | copy-start | bytes 6148
  208.6 4.4 %copy-start.63 = (f32[1,512]{1,0:T(1,128)S(1)}, f32[1,512]{1,0:T(1,128)}, u32[]{:S(2)}) copy-start(f32[1,512]{1,0:T(1,128)} %slice.1191) | copy-start | bytes 6148
  232.2 65.7 %copy-start.79 = (f32[2,512]{1,0:T(2,128)S(1)}, f32[2,512]{1,0:T(2,128)}, u32[]{:S(2)}) copy-start(f32[2,512]{1,0:T(2,128)} %param.23) | copy-start | bytes 12292
  241.2 58.4 %copy-start.77 = (f32[12,32]{1,0:T(8,128)S(1)}, f32[12,32]{1,0:T(8,128)}, u32[]{:S(2)}) copy-start(f32[12,32]{1,0:T(8,128)} %multiply_convert_fusion) | copy-start | bytes 4612
  241.2 58.4 %copy-start.84 = (s32[32]{0:T(128)S(1)}, s32[32]{0:T(128)}, u32[]{:S(2)}) copy-start(s32[32]{0:T(128)} %get-tuple-element.115) | copy-start | bytes 388
  241.2 58.4 %copy-start.85 = (s32[32]{0:T(128)S(1)}, s32[32]{0:T(128)}, u32[]{:S(2)}) copy-start(s32[32]{0:T(128)} %get-tuple-element.116) | copy-start | bytes 388
  242.7 62.6 %all-to-all-start.1 = ((f32[64,2,512]{2,1,0:T(2,128)}), f32[64,2,512]{2,1,0:T(2,128)S(1)}, u32[]{:S(2)}, u32[]{:S(2)}) async-start(f32[64,2,512]{2,1,0:T(2,128)} %broadcast_in_dim.26), calls=%async_computation.1 | async-start | bytes 524288 | tf_op jit(solution)/shard_map/all_to_all | solution.py:18
  300.7 4.8 %copy-start.81 = (pred[64]{0:T(512)(128)(4,1)S(1)}, pred[64]{0:T(512)(128)(4,1)}, u32[]{:S(2)}) copy-start(pred[64]{0:T(512)(128)(4,1)} %iota_compare_fusion.3) | copy-start | bytes 196
  (30 other events, 50.4 us)
Sparse Core Ops, SparseCore 0:
  10.1 81.8 all-gather.8
  94.8 76.1 all-gather.10
where the time goes:
time: 339 us; the launch traced here: 336 us
  local copies, waits for them, and re-layouts  113 us (33%)
  waiting for transfers between devices  70.2 us (21%)
  blocking collectives  57.1 us (17%)
  other arithmetic  31 us (9%)
  starting transfers between devices  29.5 us (9%)
  matrix products  19.8 us (6%)
  between operations  15.8 us (5%)
    slice x118, local copies, waits for them, and re-layouts, per_device(): lax.associative_scan(link_pair, (keep_rate, drive_term), reverse=directio...  67.2 us
    all_gather x1, waiting for transfers between devices, sent_together(): filled, at, outs = (lax.all_gather(both, axis, axis=dim, tiled=True), 0, [])  55.2 us
    all_gather x3, blocking collectives, collected_together(): both, at, found = (lax.all_gather(jnp.concatenate(lines), axis), 0, {})  40.3 us
    all_to_all x2, starting transfers between devices, copy_for_each(): lax.all_to_all(jnp.broadcast_to(array[None], (count, *array.shape)), axis...  19.2 us
    all_to_all x1, blocking collectives, sent_and_summed(): tiles = lax.all_to_all(in_blocks(array, dim, count), axis, 0, 0, tiled=True)  16.8 us
    pad x60, local copies, waits for them, and re-layouts, per_device(): lax.associative_scan(link_pair, (keep_rate, drive_term), reverse=directio...  15.9 us
    all_to_all x2, waiting for transfers between devices, copy_for_each(): lax.all_to_all(jnp.broadcast_to(array[None], (count, *array.shape)), axis...  14.9 us
    rev x2, local copies, waits for them, and re-layouts, per_device(): lax.associative_scan(link_pair, (keep_rate, drive_term), reverse=directio...  13.7 us
  transfers between devices with their start and end apart: 8, of which 2 were waited for; matrix products, arithmetic and copies ran while one was open for 45% of the time, Pallas kernels for 0%

commit v1 on v0

v1 whole, which is shorter than its diff:
```python
import functools

import jax
import jax.numpy as jnp
from jax import lax
from jax.experimental import pallas as pl
from jax.experimental.pallas import tpu as pltpu
from jax.sharding import Mesh
from jax.sharding import PartitionSpec as P

GRID_W = 32
REACH = 8
EPS = 1e-06
SP = ("sp_0", "sp_1", "sp_2")
SP_TP = ("sp_0", "sp_1", "sp_2", "tp")
NZ, NX, NC, NY = 8, 4, 2, 4
TOK = 384
D = 2048
CH = 512
SEGS = 8
SEG = TOK // SEGS
OWN = REACH * GRID_W
EXT = TOK + 2 * OWN
PAD = 16
OUT_ROWS = TOK // NY
N_DMA = 176
N_LOCAL = 8
F32 = jnp.float32
BF16 = jnp.bfloat16
NT = (((1,), (1,)), ((), ()))


class Links:
    def __init__(self, send, recv):
        self.send, self.recv, self.used, self.sent = send, recv, 0, []

    def slot(self):
        self.used += 1
        return self.used - 1

    def put(self, src, dst, slot, **dev):
        copy = pltpu.make_async_remote_copy(
            src_ref=src,
            dst_ref=dst,
            send_sem=self.send.at[slot],
            recv_sem=self.recv.at[slot],
            device_id=dev,
            device_id_type=pl.DeviceIdType.MESH,
        )
        copy.start()
        self.sent.append(copy)

    def got(self, region, slot, **dev):
        pltpu.make_async_remote_copy(
            src_ref=region,
            dst_ref=region,
            send_sem=self.send.at[slot],
            recv_sem=self.recv.at[slot],
            device_id=dev,
            device_id_type=pl.DeviceIdType.MESH,
        ).wait_recv()

    def drain(self):
        for copy in self.sent:
            copy.wait_send()


def weight_gather(links, buf, z, x, c):
    lo, hi = pl.ds(0, 16), pl.ds(16, 16)

    def zz(d):
        return lax.rem(z + (d + NZ), NZ)

    def xx(d):
        return lax.rem(x + (d + NX), NX)

    other = {"sp_2": 1 - c}
    a1 = {dx: links.slot() for dx in (1, 3, 2)}
    a2 = {
        (s, k, g): links.slot()
        for s in (1, -1)
        for g in (0, 1)
        for k in range(1, (5 if (s == 1) == (g == 0) else 4))
    }
    b1 = {(s, k): links.slot() for s in (1, -1) for k in range(1, 5 if s == 1 else 4)}
    rel = [0, -1, 1, -2, 2, -3, 3, 4]
    b2 = {(d, s): links.slot() for d in rel for s in (1, -1)}
    b3 = {d: links.slot() for d in rel}
    dd = {d: links.slot() for d in rel}

    def pair(d, g):
        return buf.at[zz(d), pl.ds(2 * g, 2), c, lo]

    def b_spread(d):
        piece = buf.at[zz(d), x, c, hi]
        for s in (1, -1):
            links.put(piece, piece, b2[d, s], sp_1=xx(s))

    def b_relay(d):
        for s in (1, -1):
            piece = buf.at[zz(d), xx(-s), c, hi]
            links.got(piece, b2[d, s], sp_1=xx(s))
            if (d % 2 == 0) == (s == 1):
                links.put(piece, piece, b3[d], sp_1=xx(s))

    def row_done(d):
        s = 1 if d % 2 == 0 else -1
        links.got(buf.at[zz(d), xx(2), c, hi], b3[d], sp_1=xx(s))
        row = buf.at[zz(d), pl.ds(0, NX), c]
        links.put(row, row, dd[d], **other)

    def first():
        own = buf.at[z, x, c, lo]
        for dx in (1, 3, 2):
            links.put(own, own, a1[dx], sp_1=xx(dx))
        own = buf.at[z, x, c, hi]
        for s in (1, -1):
            links.put(own, own, b1[s, 1], sp_0=zz(s))
        b_spread(0)

    def second():
        for dx in (1, 3, 2):
            links.got(buf.at[z, xx(-dx), c, lo], a1[dx], sp_1=xx(dx))
        for g in (0, 1):
            for s in (1, -1):
                links.put(pair(0, g), pair(0, g), a2[s, 1, g], sp_0=zz(s))

    def hop(k):
        for s in (1, -1):
            if (s, k) in b1:
                piece = buf.at[zz(-s * k), x, c, hi]
                links.got(piece, b1[s, k], sp_0=zz(s))
                if (s, k + 1) in b1:
                    links.put(piece, piece, b1[s, k + 1], sp_0=zz(s))
                b_spread(-s * k if k < 4 else 4)
        for g in (0, 1):
            for s in (1, -1):
                if (s, k, g) in a2:
                    piece = pair(-s * k, g)
                    links.got(piece, a2[s, k, g], sp_0=zz(s))
                    if (s, k + 1, g) in a2:
                        links.put(piece, piece, a2[s, k + 1, g], sp_0=zz(s))
        if k == 1:
            b_relay(0)
        else:
            b_relay(-(k - 1))
            b_relay(k - 1)
        if k == 2:
            row_done(0)
        if k > 2:
            row_done(-(k - 2))
            row_done(k - 2)

    def last():
        b_relay(4)
        for d in (-3, 3, 4):
            row_done(d)

    def arrived():
        for d in rel:
            links.got(buf.at[zz(d), pl.ds(0, NX), 1 - c], dd[d], **other)

    return [first, second] + [functools.partial(hop, k) for k in (1, 2, 3, 4)] + [last, arrived]


def logistic(v):
    return 1.0 / (1.0 + jnp.exp(-v))


def one_minus_exp(y, e):
    series = 1.0 + y * (1.0 / 8.0)
    for n in (7, 6, 5, 4, 3, 2):
        series = 1.0 + y * (1.0 / n) * series
    return jnp.where(y > -0.3, -y * series, 1.0 - e)


def layer(
    tokens, gain, wpi, wli, pmix, taps, rgate, igate, decay, logd, start, wop, wol, out,
    tok, nrm, win, wout, pmv, rgv, igv, box, rcp, ulb, ulf, hb, cvb, pext, pdf, gs, aa, bb,
    sg, ex, c1, c2, ycat, part, rs1, rs2, rs3, mg, send, recv, local,
):
    z, x, c = (lax.axis_index(n) for n in SP)
    y = lax.axis_index("tp")
    s = (z * NX + x) * NC + c
    links = Links(send, recv)

    def zz(d):
        return lax.rem(z + (d + NZ), NZ)

    def xx(d):
        return lax.rem(x + (d + NX), NX)

    def yy(d):
        return lax.rem(y + (d + NY), NY)

    def run_dev(d):
        t = lax.rem(s + (d + NZ * NX * NC), NZ * NX * NC)
        return {"sp_0": t // (NX * NC), "sp_1": lax.rem(t // NC, NX), "sp_2": lax.rem(t, NC)}

    after, before = run_dev(1), run_dev(-1)

    loads = [
        pltpu.make_async_copy(tokens, tok.at[y], local.at[0]),
        pltpu.make_async_copy(wpi, win.at[z, x, c, :, pl.ds(0, CH)], local.at[1]),
        pltpu.make_async_copy(wli, win.at[z, x, c, :, pl.ds(CH, CH)], local.at[2]),
        pltpu.make_async_copy(pmix, pmv, local.at[3]),
        pltpu.make_async_copy(rgate, rgv, local.at[4]),
        pltpu.make_async_copy(igate, igv, local.at[5]),
    ]
    for load in loads:
        load.start()

    barrier = pltpu.get_barrier_semaphore()
    peers = [{"tp": yy(1)}, {"tp": yy(-1)}, after, before]
    peers += [{"sp_0": zz(d)} for d in range(1, NZ)]
    around = [(dx, dc) for dx in range(NX) for dc in range(NC) if dx or dc]
    for dx, dc in around:
        peers.append({"sp_1": xx(dx), "sp_2": lax.rem(c + dc, NC)})
    for peer in peers:
        pl.semaphore_signal(barrier, inc=1, device_id=peer, device_id_type=pl.DeviceIdType.MESH)

    eye = (
        lax.broadcasted_iota(jnp.int32, (32, 32), 0) == lax.broadcasted_iota(jnp.int32, (32, 32), 1)
    ).astype(BF16)
    for k, w in enumerate((wop, wol)):
        turned = lax.dot_general(eye, w[...], NT, preferred_element_type=F32)
        wout[z, x, c, :, k * CH : (k + 1) * CH] = turned.astype(BF16)

    pl.semaphore_wait(barrier, len(peers))
    for load in loads[:3]:
        load.wait()

    halves = (pl.ds(0, TOK // 2), pl.ds(TOK // 2, TOK // 2))
    t1 = {(d, h): links.slot() for d in (1, -1) for h in (0, 1)}
    t2 = {d: links.slot() for d in (1, -1)}
    for i in (0, 1):
        for d in (1, -1):
            h = i if d == 1 else 1 - i
            piece = tok.at[y, halves[h]]
            links.put(piece, piece, t1[d, h], tp=yy(d))
    w_in = weight_gather(links, win, z, x, c)
    w_out = weight_gather(links, wout, z, x, c)
    w_in[0]()

    def token_relay():
        for d, h in ((1, 0), (-1, 1)):
            piece = tok.at[yy(-d), halves[h]]
            links.got(piece, t1[d, h], tp=yy(d))
            links.put(piece, piece, t2[d], tp=yy(d))

    half = lax.shift_left(jnp.int32(1), y)
    grid_rows = TOK // GRID_W
    row_count = grid_rows * NZ * NX * NC
    first_row = s * grid_rows

    def boxes(i, _):
        at = pl.multiple_of(i * 32, 32)
        er = lax.shift_right_logical(lax.broadcasted_iota(jnp.int32, (32, EXT), 1), 5)
        ec = lax.broadcasted_iota(jnp.int32, (32, EXT), 1) & (GRID_W - 1)
        col = lax.broadcasted_iota(jnp.int32, (32, EXT), 0)
        low = jnp.maximum(i - half, -first_row) + REACH
        high = jnp.minimum(i + half, row_count - first_row) + REACH
        inside = (er >= low) & (er < high) & (ec >= col - half) & (ec < col + half)
        box[pl.ds(at, 32), :] = jnp.where(inside, 1.0, 0.0).astype(BF16)
        cc = lax.broadcasted_iota(jnp.int32, (32, 128), 0)
        cols = jnp.minimum(cc + half, GRID_W) - jnp.maximum(cc - half, 0)
        rcp[pl.ds(at, 32), :] = 1.0 / (cols * (high - low)).astype(F32)
        return 0

    lax.fori_loop(0, grid_rows, boxes, 0)

    w_in[1]()
    w_in[2]()
    token_relay()
    for step in w_in[3:7]:
        step()
    w_out[0]()
    for d, h in ((1, 1), (-1, 0)):
        links.got(tok.at[yy(-d), halves[h]], t1[d, h], tp=yy(d))
    for d, h in ((1, 0), (-1, 1)):
        links.got(tok.at[yy(2), halves[h]], t2[d], tp=yy(d))

    def norm(i, _):
        rows = pl.ds(pl.multiple_of(i * 32, 32), 32)
        total = jnp.zeros((32, 1), F32)
        for k in range(NY):
            v = tok[k, rows, :].astype(F32)
            total = total + jnp.sum(v * v, axis=1, keepdims=True)
        scale = lax.rsqrt(total * (1.0 / D) + EPS)
        for k in range(NY):
            cols = slice(k * CH, (k + 1) * CH)
            v = tok[k, rows, :].astype(F32)
            nrm[rows, cols] = (v * scale * gain[:, cols]).astype(BF16)
        return 0

    lax.fori_loop(0, TOK // 32, norm, 0)
    w_in[7]()
    w_out[1]()

    def project(col):
        w = win[:, :, :, :, col : col + 256].reshape(D, 256)
        return jnp.dot(nrm[...], w, preferred_element_type=F32).astype(BF16)

    for n in range(2):
        u = project(CH + n * 256)
        ulb[:, n * 256 : (n + 1) * 256] = u
        for k in range(2):
            ulf[2 * n + k, PAD : PAD + TOK, :] = u[:, k * 128 : (k + 1) * 128].astype(F32)
    ch = {d: links.slot() for d in (1, -1)}
    links.put(ulb.at[pl.ds(TOK - PAD, PAD)], hb.at[0], ch[1], **after)
    links.put(ulb.at[pl.ds(0, PAD)], hb.at[1], ch[-1], **before)
    for n in range(2):
        pext[OWN : OWN + TOK, n * 256 : (n + 1) * 256] = project(n * 256)
    ph = {d: links.slot() for d in (1, -1)}
    links.put(pext.at[pl.ds(TOK, OWN)], pext.at[pl.ds(0, OWN)], ph[1], **after)
    links.put(pext.at[pl.ds(OWN, OWN)], pext.at[pl.ds(OWN + TOK, OWN)], ph[-1], **before)
    w_out[2]()

    links.got(hb.at[0], ch[1], **after)
    links.got(hb.at[1], ch[-1], **before)
    has_before = jnp.where(s > 0, 1.0, 0.0).astype(F32)
    has_after = jnp.where(s < NZ * NX * NC - 1, 1.0, 0.0).astype(F32)
    for b in range(4):
        lanes = slice(b * 128, (b + 1) * 128)
        ulf[b, 0:PAD, :] = hb[0, :, lanes].astype(F32) * has_before
        ulf[b, PAD + TOK :, :] = hb[1, :, lanes].astype(F32) * has_after
    for load in loads[4:6]:
        load.wait()

    def block(b):
        lanes = slice(b * 128, (b + 1) * 128)
        tap = taps[:, lanes].astype(F32)
        acc = ulf[b, PAD - 2 : PAD - 2 + TOK, :] * tap[0:1]
        for k in range(1, 4):
            acc = acc + ulf[b, PAD - 2 + k : PAD - 2 + k + TOK, :] * tap[k : k + 1]
        conv = acc.astype(BF16)
        cvb[...] = conv.astype(F32)
        for d in range(2):
            gs[2 * d] = jnp.dot(conv, rgv[d, b], preferred_element_type=F32)
            gs[2 * d + 1] = jnp.dot(conv, igv[d, b], preferred_element_type=F32)

        def rows_of(i, _):
            rows = pl.ds(pl.multiple_of(i * 32, 32), 32)
            value = cvb[rows, :]
            for d in range(2):
                rate = logistic(gs[2 * d, rows, :])
                gate = logistic(gs[2 * d + 1, rows, :])
                keep_log = -8.0 * rate * decay[d : d + 1, lanes] + logd[d, rows, :]
                keep = jnp.exp(keep_log)
                rest = one_minus_exp(2.0 * keep_log, keep * keep)
                aa[d, b, rows, :] = keep
                bb[d, b, rows, :] = jnp.sqrt(rest) * gate * value
            return 0

        lax.fori_loop(0, TOK // 32, rows_of, 0)

    block(0)
    w_out[3]()
    block(1)
    block(2)
    w_out[4]()
    block(3)

    def scan_step(t, carry):
        new = []
        for d in range(2):
            at = pl.ds(t if d == 0 else SEG - 1 - t, SEGS, stride=SEG)
            for b in range(4):
                prod, state = carry[2 * (4 * d + b)], carry[2 * (4 * d + b) + 1]
                keep = aa[d, b, at, :]
                state = keep * state + bb[d, b, at, :]
                prod = prod * keep
                aa[d, b, at, :] = prod
                bb[d, b, at, :] = state
                new += [prod, state]
        return tuple(new)

    ones, zeros = jnp.ones((SEGS, 128), F32), jnp.zeros((SEGS, 128), F32)
    ends = lax.fori_loop(0, SEG, scan_step, (ones, zeros) * 8, unroll=2)
    for d in range(2):
        for b in range(4):
            for k in range(2):
                sg[k, d, :, b * 128 : (b + 1) * 128] = ends[2 * (4 * d + b) + k]
    me = x * NC + c
    for d in range(2):
        prod, state = jnp.ones((1, CH), F32), jnp.zeros((1, CH), F32)
        for j in range(SEGS) if d == 0 else reversed(range(SEGS)):
            ex[0, d, j : j + 1, :] = prod
            ex[1, d, j : j + 1, :] = state
            keep = sg[0, d, j : j + 1, :]
            state = keep * state + sg[1, d, j : j + 1, :]
            prod = prod * keep
        c1[me, 2 * d : 2 * d + 1, :] = prod
        c1[me, 2 * d + 1 : 2 * d + 2, :] = state
    k1 = {p: links.slot() for p in around}
    for dx, dc in around:
        links.put(
            c1.at[me], c1.at[me], k1[dx, dc], sp_1=xx(dx), sp_2=lax.rem(c + dc, NC)
        )
    w_out[5]()

    loads[3].wait()
    links.got(pext.at[pl.ds(0, OWN)], ph[1], **after)
    links.got(pext.at[pl.ds(OWN + TOK, OWN)], ph[-1], **before)

    def combine(table, mine):
        full, inside = [], []
        for d in range(2):
            count = NZ
            prod, state = jnp.ones((1, CH), F32), jnp.zeros((1, CH), F32)
            in_p, in_s = prod, state
            for k in range(count) if d == 0 else reversed(range(count)):
                keep = table[k, 2 * d : 2 * d + 1, :]
                state = keep * state + table[k, 2 * d + 1 : 2 * d + 2, :]
                prod = prod * keep
                passed = (k < mine) if d == 0 else (k > mine)
                in_p = jnp.where(passed, prod, in_p)
                in_s = jnp.where(passed, state, in_s)
            full.append((prod, state))
            inside.append((in_p, in_s))
        return full, inside

    def pooled(n):
        cols = slice(n * 256, (n + 1) * 256)
        total = jnp.dot(box[...], pext[:, cols], preferred_element_type=F32)
        own = pext[OWN : OWN + TOK, cols].astype(F32)
        scale = jnp.concatenate([rcp[...], rcp[...]], axis=1)
        pdf[:, cols] = (total * scale - own).astype(BF16)

    for n in range(2):
        pooled(n)

    for dx, dc in around:
        links.got(
            c1.at[xx(-dx) * NC + lax.rem(c + dc, NC)],
            k1[dx, dc],
            sp_1=xx(dx),
            sp_2=lax.rem(c + dc, NC),
        )
    full, near = combine(c1, me)
    for d in range(2):
        c2[z, 2 * d : 2 * d + 1, :] = full[d][0]
        c2[z, 2 * d + 1 : 2 * d + 2, :] = full[d][1]
    k2 = {d: links.slot() for d in range(1, NZ)}
    for d in range(1, NZ):
        links.put(c2.at[z], c2.at[z], k2[d], sp_0=zz(d))
    w_out[6]()

    for n in range(2):
        cols = slice(n * 256, (n + 1) * 256)
        ycat[:, cols] = jnp.dot(pdf[...], pmv[0, :, cols], preferred_element_type=F32).astype(BF16)

    for d in range(1, NZ):
        links.got(c2.at[zz(-d)], k2[d], sp_0=zz(d))
    _, far = combine(c2, z)
    for d in range(2):
        (np_, ns_), (fp_, fs_) = near[d], far[d]
        enter = np_ * fs_ + ns_ + (np_ * fp_) * start[d : d + 1, :]
        ex[0, d] = ex[1, d] + ex[0, d] * enter
    for j in range(SEGS):
        rows = slice(j * SEG, (j + 1) * SEG)
        for b in range(4):
            lanes = slice(b * 128, (b + 1) * 128)
            h0 = bb[0, b, rows, :] + aa[0, b, rows, :] * ex[0, 0, j : j + 1, lanes]
            h1 = bb[1, b, rows, :] + aa[1, b, rows, :] * ex[0, 1, j : j + 1, lanes]
            ycat[rows, CH + b * 128 : CH + (b + 1) * 128] = (h0 + h1).astype(BF16)
    w_out[7]()

    q1 = [links.slot() for _ in range(NZ)]
    q2 = [links.slot() for _ in range(NZ)]
    q3 = [links.slot() for _ in range(NZ)]

    def relay(n):
        cols = slice(n * 256, (n + 1) * 256)
        d = 1 if n % 2 == 0 else -1
        at = rs2.at[:, pl.ds(n * 256, 256)]
        links.got(at, q2[n], tp=yy(d))
        mg[:, cols] = (rs2[:, cols].astype(F32) + part[yy(d), :, cols].astype(F32)).astype(BF16)
        there = pl.ds(n * 256, 256)
        links.put(mg.at[:, there], rs3.at[:, there], q3[n], tp=yy(d))

    for n in range(NZ):
        cols = slice(n * 256, (n + 1) * 256)
        there = pl.ds(n * 256, 256)
        w = wout[n].reshape(256, 2 * CH)
        acc = lax.dot_general(ycat[...], w, NT, preferred_element_type=F32)
        for k in range(NY):
            part[k, :, cols] = acc[k * OUT_ROWS : (k + 1) * OUT_ROWS].astype(BF16)
        d = 1 if n % 2 == 0 else -1
        links.put(part.at[yy(2), :, there], rs2.at[:, there], q2[n], tp=yy(d))
        links.put(part.at[yy(-d), :, there], rs1.at[:, there], q1[n], tp=yy(-d))
        if n >= 2:
            relay(n - 2)
    relay(NZ - 2)
    relay(NZ - 1)
    for n in range(NZ):
        cols = slice(n * 256, (n + 1) * 256)
        there = pl.ds(n * 256, 256)
        d = 1 if n % 2 == 0 else -1
        links.got(rs1.at[:, there], q1[n], tp=yy(-d))
        links.got(rs3.at[:, there], q3[n], tp=yy(d))
        total = part[y, :, cols].astype(F32) + rs1[:, cols].astype(F32) + rs3[:, cols].astype(F32)
        out[:, cols] = total.astype(BF16)
    links.drain()


def per_device(
    tokens, norm_gain, w_pool_in, w_lru_in, pool_mix, conv_taps, rec_gate, in_gate, decay_rate,
    log_decay, start_state, w_out_pool, w_out_lru,
):
    spread = jnp.broadcast_to(log_decay[:, :, None], (2, TOK, 128))
    anywhere = pl.BlockSpec(memory_space=pl.ANY)
    near = pl.BlockSpec(memory_space=pltpu.VMEM)
    buf = pltpu.VMEM
    return pl.pallas_call(
        layer,
        out_shape=jax.ShapeDtypeStruct((OUT_ROWS, D), BF16),
        in_specs=[
            anywhere, near, anywhere, anywhere, anywhere, near, anywhere, anywhere, near, near,
            near, near, near,
        ],
        out_specs=near,
        scratch_shapes=[
            buf((NY, TOK, CH), BF16),
            buf((TOK, D), BF16),
            buf((NZ, NX, NC, 32, 2 * CH), BF16),
            buf((NZ, NX, NC, 32, 2 * CH), BF16),
            buf((1, CH, CH), BF16),
            buf((2, 4, 128, 128), BF16),
            buf((2, 4, 128, 128), BF16),
            buf((TOK, EXT), BF16),
            buf((TOK, 128), F32),
            buf((TOK, CH), BF16),
            buf((4, TOK + 2 * PAD, 128), F32),
            buf((2, PAD, CH), BF16),
            buf((TOK, 128), F32),
            buf((EXT, CH), BF16),
            buf((TOK, CH), BF16),
            buf((4, TOK, 128), F32),
            buf((2, 4, TOK, 128), F32),
            buf((2, 4, TOK, 128), F32),
            buf((2, 2, SEGS, CH), F32),
            buf((2, 2, SEGS, CH), F32),
            buf((NX * NC, 4, CH), F32),
            buf((NZ, 4, CH), F32),
            buf((TOK, 2 * CH), BF16),
            buf((NY, OUT_ROWS, D), BF16),
            buf((OUT_ROWS, D), BF16),
            buf((OUT_ROWS, D), BF16),
            buf((OUT_ROWS, D), BF16),
            buf((OUT_ROWS, D), BF16),
            pltpu.SemaphoreType.DMA((N_DMA,)),
            pltpu.SemaphoreType.DMA((N_DMA,)),
            pltpu.SemaphoreType.DMA((N_LOCAL,)),
        ],
        compiler_params=pltpu.CompilerParams(
            collective_id=0, has_side_effects=True, vmem_limit_bytes=60 * 1024 * 1024
        ),
        name="layer",
    )(
        tokens, norm_gain.reshape(1, D), w_pool_in, w_lru_in, pool_mix, conv_taps, rec_gate,
        in_gate, decay_rate, spread, start_state, w_out_pool, w_out_lru,
    )


def solution(mesh):
    torus = Mesh(mesh.devices.reshape(NZ, NX, NC, mesh.shape["tp"]), SP_TP)
    in_specs = (
        P(SP, "tp"),
        P(),
        P(SP, "tp"),
        P(SP, "tp"),
        P("tp", None, None),
        P(None, "tp"),
        P(None, "tp", None, None),
        P(None, "tp", None, None),
        P(None, "tp"),
        P(None, SP),
        P(None, "tp"),
        P("tp", SP),
        P("tp", SP),
    )
    return jax.shard_map(
        per_device, mesh=torus, in_specs=in_specs, out_specs=P(SP_TP, None), check_vma=False
    )
```

time: 339 us -> 93.1 us (0.27)
  local copies, waits for them, and re-layouts: 113 us -> 4.95 us
  Pallas kernels: 0 us -> 87.6 us
  waiting for transfers between devices: 70.2 us -> 0 us
  blocking collectives: 57.1 us -> 0 us
  other arithmetic: 31 us -> 0 us
  starting transfers between devices: 29.5 us -> 0 us
  matrix products: 19.8 us -> 0 us
  between operations: 15.8 us -> 0.01 us
    pallas_call x0 -> x1, Pallas kernels: none -> 87.6 us  [per_device(): pl.pallas_call(layer, out_shape=jax.ShapeDtypeStruct((OUT_ROWS, D), BF16)...]
    slice x149 -> x0, local copies, waits for them, and re-layouts: 70 us -> none  [the longest x118 67.2 us: per_device(): lax.associative_scan(link_pair, (keep_rate, drive_term), reverse=directio...]
    all_gather x2 -> x0, waiting for transfers between devices: 55.2 us -> none  [the longest x1 55.2 us: sent_together(): filled, at, outs = (lax.all_gather(both, axis, axis=dim, tiled=True), 0, [])]
    all_gather x3 -> x0, blocking collectives: 40.3 us -> none  [collected_together(): both, at, found = (lax.all_gather(jnp.concatenate(lines), axis), 0, {})]
    dot_general x10 -> x0, matrix products: 19.8 us -> none  [the longest x1 4.52 us: per_device(): jnp.dot(y_pool, weight_pool, preferred_element_type=jnp.float32)]
    all_to_all x2 -> x0, starting transfers between devices: 19.2 us -> none  [copy_for_each(): lax.all_to_all(jnp.broadcast_to(array[None], (count, *array.shape)), axis...]
    all_to_all x1 -> x0, blocking collectives: 16.8 us -> none  [sent_and_summed(): tiles = lax.all_to_all(in_blocks(array, dim, count), axis, 0, 0, tiled=True)]
    pad x60 -> x0, local copies, waits for them, and re-layouts: 15.9 us -> none  [per_device(): lax.associative_scan(link_pair, (keep_rate, drive_term), reverse=directio...]
  transfers between devices with their start and end apart: 8 -> 0, of which waited for: 2 -> 0; matrix products, arithmetic and copies ran while one was open for 45% -> 0% of each run, Pallas kernels for 0% -> 0%
where the time goes in v1:
time: 93.1 us; the launch traced here: 92.6 us
  Pallas kernels  87.6 us (94%)
  local copies, waits for them, and re-layouts  4.95 us (5%)
    pallas_call x1, Pallas kernels, per_device(): pl.pallas_call(layer, out_shape=jax.ShapeDtypeStruct((OUT_ROWS, D), BF16)...  87.6 us
    unnamed x7, local copies, waits for them, and re-layouts  4.04 us

profile of v1, /device:TPU:8, one launch (start us, length us, event | category | flops | bytes accessed | tf_op | source)
XLA Modules:
  0.0 92.6 jit_solution(3088553210641924665)
XLA Ops:
  0.0 0.0 copy-start
  0.0 1.5 %copy.14.wop = bf16[512,32]{1,0:T(8,128)(2,1)} copy(bf16[512,32]{0,1:T(8,128)(2,1)} %param.24) | data formatting | bytes 65536 | tf_op args[11]
  1.5 0.0 copy-done
  1.5 0.0 copy-start.1
  1.5 0.8 copy.15.wol
  2.3 0.0 copy-done.1
  2.3 0.9 broadcast_in_dim.2.logd
  3.2 87.6 %layer.1 = bf16[96,2048]{1,0:T(8,128)(2,1)} custom-call(bf16[384,512]{1,0:T(8,128)(2,1)} %tokens.1, f32[1,2048]{1,0:T(1,128)} %bitcast.1, bf16[32,512]{1,0:T(8,128)(2,1)} %wpi.1, bf16[32,512]{1,0:T(8,128)(2,1)} %wli.1, bf16[1,512,512]{2,1,0:T(8,128)(2,1)} %pmix.1, bf16[4,512]{1,0:T(4,128)(2,1)} %taps.1, bf16[2,4,128,128]{3,2,1,0:T(8,128)(2,1)} %rgate.1, ...), custom_call_target="tpu_custom_call" | custom-call | tf_op jit(solution)/shard_map/layer/pallas_call | solution.py:515
  90.8 1.8 %copy.17 = bf16[96,2048]{1,0:T(8,128)(2,1)} copy(bf16[96,2048]{1,0:T(8,128)(2,1)} %layer.1) | data formatting | bytes 786432
Async XLA Ops:
  0.0 1.5 %copy-start = (bf16[512,32]{0,1:T(8,128)(2,1)S(1)}, bf16[512,32]{0,1:T(8,128)(2,1)}, u32[]{:S(2)}) copy-start(bf16[512,32]{0,1:T(8,128)(2,1)} %param.25) | copy-start | bytes 98308
  1.5 0.8 copy-start.1

commit v2 on v1

--- a/solution.py
+++ b/solution.py
@@ -23,7 +23,7 @@
 EXT = TOK + 2 * OWN
 PAD = 16
 OUT_ROWS = TOK // NY
-N_DMA = 176
+N_DMA = 192
 N_LOCAL = 8
 F32 = jnp.float32
 BF16 = jnp.bfloat16
@@ -75,29 +75,53 @@
         return lax.rem(x + (d + NX), NX)
 
     other = {"sp_2": 1 - c}
+    both = (1, -1)
+    rel = [0, -1, 1, -2, 2, -3, 3, 4]
     a1 = {dx: links.slot() for dx in (1, 3, 2)}
     a2 = {
-        (s, k, g): links.slot()
-        for s in (1, -1)
-        for g in (0, 1)
-        for k in range(1, (5 if (s == 1) == (g == 0) else 4))
+        (s, k, e): links.slot()
+        for s in both
+        for e in range(NX)
+        for k in range(1, 5 if (s == 1) == (e < 2) else 4)
     }
-    b1 = {(s, k): links.slot() for s in (1, -1) for k in range(1, 5 if s == 1 else 4)}
-    rel = [0, -1, 1, -2, 2, -3, 3, 4]
-    b2 = {(d, s): links.slot() for d in rel for s in (1, -1)}
+    b1 = {(s, k): links.slot() for s in both for k in range(1, 5 if s == 1 else 4)}
+    b2 = {(d, s): links.slot() for d in rel for s in both}
     b3 = {d: links.slot() for d in rel}
     dd = {d: links.slot() for d in rel}
 
-    def pair(d, g):
-        return buf.at[zz(d), pl.ds(2 * g, 2), c, lo]
+    def a_send(s, k, e):
+        if (s, k, e) in a2:
+            piece = buf.at[zz(-s * (k - 1)), xx(e), c, lo]
+            links.put(piece, piece, a2[s, k, e], sp_0=zz(s))
+
+    def a_hop(s, k, e):
+        if (s, k, e) in a2:
+            links.got(buf.at[zz(-s * k), xx(e), c, lo], a2[s, k, e], sp_0=zz(s))
+            a_send(s, k + 1, e)
+
+    def a_side(dx):
+        links.got(buf.at[z, xx(-dx), c, lo], a1[dx], sp_1=xx(dx))
+        for s in both:
+            a_send(s, 1, NX - dx)
+
+    def b_send(s, k):
+        if (s, k) in b1:
+            piece = buf.at[zz(-s * (k - 1)), x, c, hi]
+            links.put(piece, piece, b1[s, k], sp_0=zz(s))
 
     def b_spread(d):
         piece = buf.at[zz(d), x, c, hi]
-        for s in (1, -1):
+        for s in both:
             links.put(piece, piece, b2[d, s], sp_1=xx(s))
 
+    def b_hop(s, k):
+        if (s, k) in b1:
+            links.got(buf.at[zz(-s * k), x, c, hi], b1[s, k], sp_0=zz(s))
+            b_send(s, k + 1)
+            b_spread(-s * k if k < 4 else 4)
+
     def b_relay(d):
-        for s in (1, -1):
+        for s in both:
             piece = buf.at[zz(d), xx(-s), c, hi]
             links.got(piece, b2[d, s], sp_1=xx(s))
             if (d % 2 == 0) == (s == 1):
@@ -113,54 +137,33 @@
         own = buf.at[z, x, c, lo]
         for dx in (1, 3, 2):
             links.put(own, own, a1[dx], sp_1=xx(dx))
-        own = buf.at[z, x, c, hi]
-        for s in (1, -1):
-            links.put(own, own, b1[s, 1], sp_0=zz(s))
+        for s in both:
+            b_send(s, 1)
+            a_send(s, 1, 0)
         b_spread(0)
-
-    def second():
-        for dx in (1, 3, 2):
-            links.got(buf.at[z, xx(-dx), c, lo], a1[dx], sp_1=xx(dx))
-        for g in (0, 1):
-            for s in (1, -1):
-                links.put(pair(0, g), pair(0, g), a2[s, 1, g], sp_0=zz(s))
-
-    def hop(k):
-        for s in (1, -1):
-            if (s, k) in b1:
-                piece = buf.at[zz(-s * k), x, c, hi]
-                links.got(piece, b1[s, k], sp_0=zz(s))
-                if (s, k + 1) in b1:
-                    links.put(piece, piece, b1[s, k + 1], sp_0=zz(s))
-                b_spread(-s * k if k < 4 else 4)
-        for g in (0, 1):
-            for s in (1, -1):
-                if (s, k, g) in a2:
-                    piece = pair(-s * k, g)
-                    links.got(piece, a2[s, k, g], sp_0=zz(s))
-                    if (s, k + 1, g) in a2:
-                        links.put(piece, piece, a2[s, k + 1, g], sp_0=zz(s))
-        if k == 1:
-            b_relay(0)
-        else:
-            b_relay(-(k - 1))
-            b_relay(k - 1)
-        if k == 2:
-            row_done(0)
-        if k > 2:
-            row_done(-(k - 2))
-            row_done(k - 2)
-
-    def last():
-        b_relay(4)
-        for d in (-3, 3, 4):
-            row_done(d)
 
     def arrived():
         for d in rel:
             links.got(buf.at[zz(d), pl.ds(0, NX), 1 - c], dd[d], **other)
 
-    return [first, second] + [functools.partial(hop, k) for k in (1, 2, 3, 4)] + [last, arrived]
+    def at(f, *args):
+        return functools.partial(f, *args)
+
+    rounds = [[first]]
+    rounds.append(
+        [at(a_side, 1), at(a_side, 3)]
+        + [at(b_hop, s, 1) for s in both]
+        + [at(a_hop, s, 1, 0) for s in both]
+        + [at(a_side, 2), at(b_relay, 0)]
+    )
+    for k in (2, 3, 4, 5):
+        turn = [at(b_hop, s, k) for s in both] + [at(a_hop, s, k, 0) for s in both]
+        turn += [at(a_hop, s, k - 1, e) for e in (3, 1, 2) for s in both]
+        turn += [at(b_relay, d) for d in ((1 - k, k - 1) if k < 5 else (4,))]
+        turn += [at(row_done, d) for d in ((0,) if k == 2 else (2 - k, k - 2))]
+        rounds.append(turn)
+    rounds.append([at(row_done, 4)])
+    return rounds, arrived
 
 
 def logistic(v):
@@ -168,15 +171,19 @@
 
 
 def one_minus_exp(y, e):
-    series = 1.0 + y * (1.0 / 8.0)
-    for n in (7, 6, 5, 4, 3, 2):
-        series = 1.0 + y * (1.0 / n) * series
-    return jnp.where(y > -0.3, -y * series, 1.0 - e)
+    series = y * (-1.0 / 720.0) - 1.0 / 120.0
+    for n in (24.0, 6.0, 2.0, 1.0):
+        series = y * series - 1.0 / n
+    return jnp.where(y > -0.125, y * series, 1.0 - e)
+
+
+def root(v):
+    return v * lax.rsqrt(jnp.maximum(v, 1e-37))
 
 
 def layer(
     tokens, gain, wpi, wli, pmix, taps, rgate, igate, decay, logd, start, wop, wol, out,
-    tok, nrm, win, wout, pmv, rgv, igv, box, rcp, ulb, ulf, hb, cvb, pext, pdf, gs, aa, bb,
+    tok, nrm, win, wout, pmv, rgv, igv, ldb, box, rcp, ulb, ulf, hb, cvb, pext, pdf, gs, aa, bb,
     sg, ex, c1, c2, ycat, part, rs1, rs2, rs3, mg, send, recv, local,
 ):
     z, x, c = (lax.axis_index(n) for n in SP)
@@ -206,6 +213,8 @@
         pltpu.make_async_copy(pmix, pmv, local.at[3]),
         pltpu.make_async_copy(rgate, rgv, local.at[4]),
         pltpu.make_async_copy(igate, igv, local.at[5]),
+        pltpu.make_async_copy(wop, wout.at[z, x, c, :, pl.ds(0, CH)], local.at[6]),
+        pltpu.make_async_copy(wol, wout.at[z, x, c, :, pl.ds(CH, CH)], local.at[7]),
     ]
     for load in loads:
         load.start()
@@ -219,35 +228,10 @@
     for peer in peers:
         pl.semaphore_signal(barrier, inc=1, device_id=peer, device_id_type=pl.DeviceIdType.MESH)
 
-    eye = (
-        lax.broadcasted_iota(jnp.int32, (32, 32), 0) == lax.broadcasted_iota(jnp.int32, (32, 32), 1)
-    ).astype(BF16)
-    for k, w in enumerate((wop, wol)):
-        turned = lax.dot_general(eye, w[...], NT, preferred_element_type=F32)
-        wout[z, x, c, :, k * CH : (k + 1) * CH] = turned.astype(BF16)
-
-    pl.semaphore_wait(barrier, len(peers))
-    for load in loads[:3]:
-        load.wait()
-
-    halves = (pl.ds(0, TOK // 2), pl.ds(TOK // 2, TOK // 2))
-    t1 = {(d, h): links.slot() for d in (1, -1) for h in (0, 1)}
-    t2 = {d: links.slot() for d in (1, -1)}
-    for i in (0, 1):
-        for d in (1, -1):
-            h = i if d == 1 else 1 - i
-            piece = tok.at[y, halves[h]]
-            links.put(piece, piece, t1[d, h], tp=yy(d))
-    w_in = weight_gather(links, win, z, x, c)
-    w_out = weight_gather(links, wout, z, x, c)
-    w_in[0]()
-
-    def token_relay():
-        for d, h in ((1, 0), (-1, 1)):
-            piece = tok.at[yy(-d), halves[h]]
-            links.got(piece, t1[d, h], tp=yy(d))
-            links.put(piece, piece, t2[d], tp=yy(d))
-
+    for d in range(2):
+        for i in range(TOK // 128):
+            rows = slice(i * 128, (i + 1) * 128)
+            ldb[d, rows, :] = jnp.broadcast_to(logd[d : d + 1, rows], (128, 128)).T
     half = lax.shift_left(jnp.int32(1), y)
     grid_rows = TOK // GRID_W
     row_count = grid_rows * NZ * NX * NC
@@ -269,12 +253,42 @@
 
     lax.fori_loop(0, grid_rows, boxes, 0)
 
-    w_in[1]()
-    w_in[2]()
+    pl.semaphore_wait(barrier, len(peers))
+    for load in loads[:3]:
+        load.wait()
+
+    halves = (pl.ds(0, TOK // 2), pl.ds(TOK // 2, TOK // 2))
+    t1 = {(d, h): links.slot() for d in (1, -1) for h in (0, 1)}
+    t2 = {d: links.slot() for d in (1, -1)}
+    for i in (0, 1):
+        for d in (1, -1):
+            h = i if d == 1 else 1 - i
+            piece = tok.at[y, halves[h]]
+            links.put(piece, piece, t1[d, h], tp=yy(d))
+    r_in, in_arrived = weight_gather(links, win, z, x, c)
+    r_out, out_arrived = weight_gather(links, wout, z, x, c)
+
+    def serve(*rounds):
+        for turn in rounds:
+            for step in turn:
+                step()
+
+    serve(r_in[0])
+
+    def token_relay():
+        for d, h in ((1, 0), (-1, 1)):
+            piece = tok.at[yy(-d), halves[h]]
+            links.got(piece, t1[d, h], tp=yy(d))
+            links.put(piece, piece, t2[d], tp=yy(d))
+
+    serve(r_in[1])
+    serve(r_in[2])
     token_relay()
-    for step in w_in[3:7]:
-        step()
-    w_out[0]()
+    serve(r_in[3], r_in[4])
+    for load in loads[6:8]:
+        load.wait()
+    serve(r_out[0])
+    serve(r_in[5], r_in[6])
     for d, h in ((1, 1), (-1, 0)):
         links.got(tok.at[yy(-d), halves[h]], t1[d, h], tp=yy(d))
     for d, h in ((1, 0), (-1, 1)):
@@ -294,8 +308,8 @@
         return 0
 
     lax.fori_loop(0, TOK // 32, norm, 0)
-    w_in[7]()
-    w_out[1]()
+    in_arrived()
+    serve(r_out[1])
 
     def project(col):
         w = win[:, :, :, :, col : col + 256].reshape(D, 256)
@@ -314,7 +328,6 @@
     ph = {d: links.slot() for d in (1, -1)}
     links.put(pext.at[pl.ds(TOK, OWN)], pext.at[pl.ds(0, OWN)], ph[1], **after)
     links.put(pext.at[pl.ds(OWN, OWN)], pext.at[pl.ds(OWN + TOK, OWN)], ph[-1], **before)
-    w_out[2]()
 
     links.got(hb.at[0], ch[1], **after)
     links.got(hb.at[1], ch[-1], **before)
@@ -345,20 +358,21 @@
             for d in range(2):
                 rate = logistic(gs[2 * d, rows, :])
                 gate = logistic(gs[2 * d + 1, rows, :])
-                keep_log = -8.0 * rate * decay[d : d + 1, lanes] + logd[d, rows, :]
+                keep_log = -8.0 * rate * decay[d : d + 1, lanes] + ldb[d, rows, :]
                 keep = jnp.exp(keep_log)
                 rest = one_minus_exp(2.0 * keep_log, keep * keep)
                 aa[d, b, rows, :] = keep
-                bb[d, b, rows, :] = jnp.sqrt(rest) * gate * value
+                bb[d, b, rows, :] = root(rest) * gate * value
             return 0
 
         lax.fori_loop(0, TOK // 32, rows_of, 0)
 
     block(0)
-    w_out[3]()
+    serve(r_out[2][:6])
     block(1)
+    serve(r_out[2][6:])
     block(2)
-    w_out[4]()
+    serve(r_out[3][:6])
     block(3)
 
     def scan_step(t, carry):
@@ -375,6 +389,7 @@
                 new += [prod, state]
         return tuple(new)
 
+    serve(r_out[3][6:])
     ones, zeros = jnp.ones((SEGS, 128), F32), jnp.zeros((SEGS, 128), F32)
     ends = lax.fori_loop(0, SEG, scan_step, (ones, zeros) * 8, unroll=2)
     for d in range(2):
@@ -397,7 +412,7 @@
         links.put(
             c1.at[me], c1.at[me], k1[dx, dc], sp_1=xx(dx), sp_2=lax.rem(c + dc, NC)
         )
-    w_out[5]()
+    serve(r_out[4])
 
     loads[3].wait()
     links.got(pext.at[pl.ds(0, OWN)], ph[1], **after)
@@ -444,12 +459,13 @@
     k2 = {d: links.slot() for d in range(1, NZ)}
     for d in range(1, NZ):
         links.put(c2.at[z], c2.at[z], k2[d], sp_0=zz(d))
-    w_out[6]()
+    serve(r_out[5])
 
     for n in range(2):
         cols = slice(n * 256, (n + 1) * 256)
         ycat[:, cols] = jnp.dot(pdf[...], pmv[0, :, cols], preferred_element_type=F32).astype(BF16)
 
+    serve(r_out[6])
     for d in range(1, NZ):
         links.got(c2.at[zz(-d)], k2[d], sp_0=zz(d))
     _, far = combine(c2, z)
@@ -464,7 +480,7 @@
             h0 = bb[0, b, rows, :] + aa[0, b, rows, :] * ex[0, 0, j : j + 1, lanes]
             h1 = bb[1, b, rows, :] + aa[1, b, rows, :] * ex[0, 1, j : j + 1, lanes]
             ycat[rows, CH + b * 128 : CH + (b + 1) * 128] = (h0 + h1).astype(BF16)
-    w_out[7]()
+    out_arrived()
 
     q1 = [links.slot() for _ in range(NZ)]
     q2 = [links.slot() for _ in range(NZ)]
@@ -508,7 +524,6 @@
     tokens, norm_gain, w_pool_in, w_lru_in, pool_mix, conv_taps, rec_gate, in_gate, decay_rate,
     log_decay, start_state, w_out_pool, w_out_lru,
 ):
-    spread = jnp.broadcast_to(log_decay[:, :, None], (2, TOK, 128))
     anywhere = pl.BlockSpec(memory_space=pl.ANY)
     near = pl.BlockSpec(memory_space=pltpu.VMEM)
     buf = pltpu.VMEM
@@ -517,7 +532,7 @@
         out_shape=jax.ShapeDtypeStruct((OUT_ROWS, D), BF16),
         in_specs=[
             anywhere, near, anywhere, anywhere, anywhere, near, anywhere, anywhere, near, near,
-            near, near, near,
+            near, anywhere, anywhere,
         ],
         out_specs=near,
         scratch_shapes=[
@@ -528,6 +543,7 @@
             buf((1, CH, CH), BF16),
             buf((2, 4, 128, 128), BF16),
             buf((2, 4, 128, 128), BF16),
+            buf((2, TOK, 128), F32),
             buf((TOK, EXT), BF16),
             buf((TOK, 128), F32),
             buf((TOK, CH), BF16),
@@ -559,7 +575,7 @@
         name="layer",
     )(
         tokens, norm_gain.reshape(1, D), w_pool_in, w_lru_in, pool_mix, conv_taps, rec_gate,
-        in_gate, decay_rate, spread, start_state, w_out_pool, w_out_lru,
+        in_gate, decay_rate, log_decay, start_state, w_out_pool.T, w_out_lru.T,
     )
 
 

time: 93.1 us -> 82.2 us (0.88)
  Pallas kernels: 87.6 us -> 79.3 us
  local copies, waits for them, and re-layouts: 4.95 us -> 1.77 us
    pallas_call x1, Pallas kernels: 87.6 us -> 79.3 us  [per_device(): pl.pallas_call(layer, out_shape=jax.ShapeDtypeStruct((OUT_ROWS, D), BF16)...]
    unnamed x7 -> x1, local copies, waits for them, and re-layouts: 4.04 us -> 1.77 us
where the time goes in v2:
time: 82.2 us; the launch traced here: 81.1 us
  Pallas kernels  79.3 us (96%)
  local copies, waits for them, and re-layouts  1.77 us (2%)
    pallas_call x1, Pallas kernels, per_device(): pl.pallas_call(layer, out_shape=jax.ShapeDtypeStruct((OUT_ROWS, D), BF16)...  79.3 us
    unnamed x1, local copies, waits for them, and re-layouts  1.77 us

profile of v2, /device:TPU:8, one launch (start us, length us, event | category | flops | bytes accessed | tf_op | source)
XLA Modules:
  0.0 81.1 jit_solution(8485062945231577755)
XLA Ops:
  0.0 79.3 %layer.1 = bf16[96,2048]{1,0:T(8,128)(2,1)} custom-call(bf16[384,512]{1,0:T(8,128)(2,1)} %tokens.1, f32[1,2048]{1,0:T(1,128)} %bitcast.5, bf16[32,512]{1,0:T(8,128)(2,1)} %wpi.1, bf16[32,512]{1,0:T(8,128)(2,1)} %wli.1, bf16[1,512,512]{2,1,0:T(8,128)(2,1)} %pmix.1, bf16[4,512]{1,0:T(4,128)(2,1)} %taps.1, bf16[2,4,128,128]{3,2,1,0:T(8,128)(2,1)} %rgate.1, ...), custom_call_target="tpu_custom_call" | custom-call | tf_op jit(solution)/shard_map/layer/pallas_call | solution.py:530
  79.3 1.8 %copy.15 = bf16[96,2048]{1,0:T(8,128)(2,1)} copy(bf16[96,2048]{1,0:T(8,128)(2,1)} %layer.1) | data formatting | bytes 786432

commit v3 on v2

--- a/solution.py
+++ b/solution.py
@@ -23,7 +23,8 @@
 EXT = TOK + 2 * OWN
 PAD = 16
 OUT_ROWS = TOK // NY
-N_DMA = 192
+N_SEND = 19
+N_RECV = 130
 N_LOCAL = 8
 F32 = jnp.float32
 BF16 = jnp.bfloat16
@@ -32,37 +33,35 @@
 
 class Links:
     def __init__(self, send, recv):
-        self.send, self.recv, self.used, self.sent = send, recv, 0, []
+        self.send, self.recv, self.groups, self.used = send, recv, [], 0
 
     def slot(self):
         self.used += 1
         return self.used - 1
 
-    def put(self, src, dst, slot, **dev):
-        copy = pltpu.make_async_remote_copy(
+    def group(self, region):
+        self.groups.append(region)
+        return len(self.groups) - 1
+
+    def copy(self, src, dst, group, slot, dev):
+        return pltpu.make_async_remote_copy(
             src_ref=src,
             dst_ref=dst,
-            send_sem=self.send.at[slot],
+            send_sem=self.send.at[group],
             recv_sem=self.recv.at[slot],
             device_id=dev,
             device_id_type=pl.DeviceIdType.MESH,
         )
-        copy.start()
-        self.sent.append(copy)
+
+    def put(self, src, dst, group, slot, **dev):
+        self.copy(src, dst, group, slot, dev).start()
 
     def got(self, region, slot, **dev):
-        pltpu.make_async_remote_copy(
-            src_ref=region,
-            dst_ref=region,
-            send_sem=self.send.at[slot],
-            recv_sem=self.recv.at[slot],
-            device_id=dev,
-            device_id_type=pl.DeviceIdType.MESH,
-        ).wait_recv()
-
-    def drain(self):
-        for copy in self.sent:
-            copy.wait_send()
+        self.copy(region, region, 0, slot, dev).wait_recv()
+
+    def drain(self, **dev):
+        for group, region in enumerate(self.groups):
+            self.copy(region, region, group, 0, dev).wait_send()
 
 
 def weight_gather(links, buf, z, x, c):
@@ -85,14 +84,18 @@
         for k in range(1, 5 if (s == 1) == (e < 2) else 4)
     }
     b1 = {(s, k): links.slot() for s in both for k in range(1, 5 if s == 1 else 4)}
-    b2 = {(d, s): links.slot() for d in rel for s in both}
-    b3 = {d: links.slot() for d in rel}
-    dd = {d: links.slot() for d in rel}
+    b2 = {d: links.slot() for d in rel}
+    dd = links.slot()
+    g_a1 = links.group(buf.at[0, pl.ds(0, 3), c, lo])
+    g_a2 = links.group(buf.at[pl.ds(0, 7), pl.ds(0, NX), c, lo])
+    g_b1 = links.group(buf.at[pl.ds(0, 7), 0, c, lo])
+    g_b2 = links.group(buf.at[pl.ds(0, NZ), pl.ds(0, 3), c, lo])
+    g_dd = links.group(buf.at[pl.ds(0, NZ), pl.ds(0, NX), c])
 
     def a_send(s, k, e):
         if (s, k, e) in a2:
             piece = buf.at[zz(-s * (k - 1)), xx(e), c, lo]
-            links.put(piece, piece, a2[s, k, e], sp_0=zz(s))
+            links.put(piece, piece, g_a2, a2[s, k, e], sp_0=zz(s))
 
     def a_hop(s, k, e):
         if (s, k, e) in a2:
@@ -107,12 +110,12 @@
     def b_send(s, k):
         if (s, k) in b1:
             piece = buf.at[zz(-s * (k - 1)), x, c, hi]
-            links.put(piece, piece, b1[s, k], sp_0=zz(s))
+            links.put(piece, piece, g_b1, b1[s, k], sp_0=zz(s))
 
     def b_spread(d):
         piece = buf.at[zz(d), x, c, hi]
-        for s in both:
-            links.put(piece, piece, b2[d, s], sp_1=xx(s))
+        for dx in (1, 3, 2):
+            links.put(piece, piece, g_b2, b2[d], sp_1=xx(dx))
 
     def b_hop(s, k):
         if (s, k) in b1:
@@ -120,46 +123,35 @@
             b_send(s, k + 1)
             b_spread(-s * k if k < 4 else 4)
 
-    def b_relay(d):
-        for s in both:
-            piece = buf.at[zz(d), xx(-s), c, hi]
-            links.got(piece, b2[d, s], sp_1=xx(s))
-            if (d % 2 == 0) == (s == 1):
-                links.put(piece, piece, b3[d], sp_1=xx(s))
-
     def row_done(d):
-        s = 1 if d % 2 == 0 else -1
-        links.got(buf.at[zz(d), xx(2), c, hi], b3[d], sp_1=xx(s))
+        links.got(buf.at[zz(d), pl.ds(0, 3), c, hi], b2[d], sp_1=xx(1))
         row = buf.at[zz(d), pl.ds(0, NX), c]
-        links.put(row, row, dd[d], **other)
+        links.put(row, row, g_dd, dd, **other)
 
     def first():
         own = buf.at[z, x, c, lo]
         for dx in (1, 3, 2):
-            links.put(own, own, a1[dx], sp_1=xx(dx))
+            links.put(own, own, g_a1, a1[dx], sp_1=xx(dx))
         for s in both:
             b_send(s, 1)
             a_send(s, 1, 0)
-        b_spread(0)
 
     def arrived():
-        for d in rel:
-            links.got(buf.at[zz(d), pl.ds(0, NX), 1 - c], dd[d], **other)
+        links.got(buf.at[pl.ds(0, NZ), pl.ds(0, NX), 1 - c], dd, **other)
 
     def at(f, *args):
         return functools.partial(f, *args)
 
-    rounds = [[first]]
+    rounds = [[first, at(b_spread, 0)]]
     rounds.append(
         [at(a_side, 1), at(a_side, 3)]
         + [at(b_hop, s, 1) for s in both]
         + [at(a_hop, s, 1, 0) for s in both]
-        + [at(a_side, 2), at(b_relay, 0)]
+        + [at(a_side, 2)]
     )
     for k in (2, 3, 4, 5):
         turn = [at(b_hop, s, k) for s in both] + [at(a_hop, s, k, 0) for s in both]
         turn += [at(a_hop, s, k - 1, e) for e in (3, 1, 2) for s in both]
-        turn += [at(b_relay, d) for d in ((1 - k, k - 1) if k < 5 else (4,))]
         turn += [at(row_done, d) for d in ((0,) if k == 2 else (2 - k, k - 2))]
         rounds.append(turn)
     rounds.append([at(row_done, 4)])
@@ -254,17 +246,19 @@
     lax.fori_loop(0, grid_rows, boxes, 0)
 
     pl.semaphore_wait(barrier, len(peers))
-    for load in loads[:3]:
+    for load in loads[:3] + loads[6:]:
         load.wait()
 
     halves = (pl.ds(0, TOK // 2), pl.ds(TOK // 2, TOK // 2))
+    g_t1 = links.group(tok.at[pl.ds(0, 2)])
+    g_t2 = links.group(tok.at[0])
     t1 = {(d, h): links.slot() for d in (1, -1) for h in (0, 1)}
     t2 = {d: links.slot() for d in (1, -1)}
     for i in (0, 1):
         for d in (1, -1):
             h = i if d == 1 else 1 - i
             piece = tok.at[y, halves[h]]
-            links.put(piece, piece, t1[d, h], tp=yy(d))
+            links.put(piece, piece, g_t1, t1[d, h], tp=yy(d))
     r_in, in_arrived = weight_gather(links, win, z, x, c)
     r_out, out_arrived = weight_gather(links, wout, z, x, c)
 
@@ -274,20 +268,21 @@
                 step()
 
     serve(r_in[0])
+    serve(r_out[0][:1])
 
     def token_relay():
         for d, h in ((1, 0), (-1, 1)):
             piece = tok.at[yy(-d), halves[h]]
             links.got(piece, t1[d, h], tp=yy(d))
-            links.put(piece, piece, t2[d], tp=yy(d))
+            links.put(piece, piece, g_t2, t2[d], tp=yy(d))
 
     serve(r_in[1])
     serve(r_in[2])
     token_relay()
-    serve(r_in[3], r_in[4])
-    for load in loads[6:8]:
-        load.wait()
-    serve(r_out[0])
+    serve(r_out[0][1:])
+    serve(r_in[3])
+    serve(r_in[4])
+    serve(r_out[1])
     serve(r_in[5], r_in[6])
     for d, h in ((1, 1), (-1, 0)):
         links.got(tok.at[yy(-d), halves[h]], t1[d, h], tp=yy(d))
@@ -308,8 +303,8 @@
         return 0
 
     lax.fori_loop(0, TOK // 32, norm, 0)
+    serve(r_out[2])
     in_arrived()
-    serve(r_out[1])
 
     def project(col):
         w = win[:, :, :, :, col : col + 256].reshape(D, 256)
@@ -320,15 +315,18 @@
         ulb[:, n * 256 : (n + 1) * 256] = u
         for k in range(2):
             ulf[2 * n + k, PAD : PAD + TOK, :] = u[:, k * 128 : (k + 1) * 128].astype(F32)
+    g_ch = links.group(hb)
     ch = {d: links.slot() for d in (1, -1)}
-    links.put(ulb.at[pl.ds(TOK - PAD, PAD)], hb.at[0], ch[1], **after)
-    links.put(ulb.at[pl.ds(0, PAD)], hb.at[1], ch[-1], **before)
+    links.put(ulb.at[pl.ds(TOK - PAD, PAD)], hb.at[0], g_ch, ch[1], **after)
+    links.put(ulb.at[pl.ds(0, PAD)], hb.at[1], g_ch, ch[-1], **before)
     for n in range(2):
         pext[OWN : OWN + TOK, n * 256 : (n + 1) * 256] = project(n * 256)
+    g_ph = links.group(pext.at[pl.ds(0, 2 * OWN)])
     ph = {d: links.slot() for d in (1, -1)}
-    links.put(pext.at[pl.ds(TOK, OWN)], pext.at[pl.ds(0, OWN)], ph[1], **after)
-    links.put(pext.at[pl.ds(OWN, OWN)], pext.at[pl.ds(OWN + TOK, OWN)], ph[-1], **before)
-
+    links.put(pext.at[pl.ds(TOK, OWN)], pext.at[pl.ds(0, OWN)], g_ph, ph[1], **after)
+    links.put(pext.at[pl.ds(OWN, OWN)], pext.at[pl.ds(OWN + TOK, OWN)], g_ph, ph[-1], **before)
+
+    serve(r_out[3])
     links.got(hb.at[0], ch[1], **after)
     links.got(hb.at[1], ch[-1], **before)
     has_before = jnp.where(s > 0, 1.0, 0.0).astype(F32)
@@ -368,11 +366,10 @@
         lax.fori_loop(0, TOK // 32, rows_of, 0)
 
     block(0)
-    serve(r_out[2][:6])
     block(1)
-    serve(r_out[2][6:])
+    serve(r_out[4][:5])
     block(2)
-    serve(r_out[3][:6])
+    serve(r_out[4][5:])
     block(3)
 
     def scan_step(t, carry):
@@ -389,7 +386,6 @@
                 new += [prod, state]
         return tuple(new)
 
-    serve(r_out[3][6:])
     ones, zeros = jnp.ones((SEGS, 128), F32), jnp.zeros((SEGS, 128), F32)
     ends = lax.fori_loop(0, SEG, scan_step, (ones, zeros) * 8, unroll=2)
     for d in range(2):
@@ -407,13 +403,11 @@
             prod = prod * keep
         c1[me, 2 * d : 2 * d + 1, :] = prod
         c1[me, 2 * d + 1 : 2 * d + 2, :] = state
-    k1 = {p: links.slot() for p in around}
+    g_k1, k1 = links.group(c1.at[pl.ds(0, 7)]), links.slot()
     for dx, dc in around:
-        links.put(
-            c1.at[me], c1.at[me], k1[dx, dc], sp_1=xx(dx), sp_2=lax.rem(c + dc, NC)
-        )
-    serve(r_out[4])
-
+        links.put(c1.at[me], c1.at[me], g_k1, k1, sp_1=xx(dx), sp_2=lax.rem(c + dc, NC))
+
+    serve(r_out[5], r_out[6])
     loads[3].wait()
     links.got(pext.at[pl.ds(0, OWN)], ph[1], **after)
     links.got(pext.at[pl.ds(OWN + TOK, OWN)], ph[-1], **before)
@@ -445,29 +439,20 @@
     for n in range(2):
         pooled(n)
 
-    for dx, dc in around:
-        links.got(
-            c1.at[xx(-dx) * NC + lax.rem(c + dc, NC)],
-            k1[dx, dc],
-            sp_1=xx(dx),
-            sp_2=lax.rem(c + dc, NC),
-        )
+    links.got(c1.at[pl.ds(0, 7)], k1, **after)
     full, near = combine(c1, me)
     for d in range(2):
         c2[z, 2 * d : 2 * d + 1, :] = full[d][0]
         c2[z, 2 * d + 1 : 2 * d + 2, :] = full[d][1]
-    k2 = {d: links.slot() for d in range(1, NZ)}
+    g_k2, k2 = links.group(c2.at[pl.ds(0, 7)]), links.slot()
     for d in range(1, NZ):
-        links.put(c2.at[z], c2.at[z], k2[d], sp_0=zz(d))
-    serve(r_out[5])
+        links.put(c2.at[z], c2.at[z], g_k2, k2, sp_0=zz(d))
 
     for n in range(2):
         cols = slice(n * 256, (n + 1) * 256)
         ycat[:, cols] = jnp.dot(pdf[...], pmv[0, :, cols], preferred_element_type=F32).astype(BF16)
 
-    serve(r_out[6])
-    for d in range(1, NZ):
-        links.got(c2.at[zz(-d)], k2[d], sp_0=zz(d))
+    links.got(c2.at[pl.ds(0, 7)], k2, **after)
     _, far = combine(c2, z)
     for d in range(2):
         (np_, ns_), (fp_, fs_) = near[d], far[d]
@@ -482,6 +467,7 @@
             ycat[rows, CH + b * 128 : CH + (b + 1) * 128] = (h0 + h1).astype(BF16)
     out_arrived()
 
+    g_q1, g_q2, g_q3 = links.group(rs1), links.group(rs2), links.group(rs3)
     q1 = [links.slot() for _ in range(NZ)]
     q2 = [links.slot() for _ in range(NZ)]
     q3 = [links.slot() for _ in range(NZ)]
@@ -493,7 +479,7 @@
         links.got(at, q2[n], tp=yy(d))
         mg[:, cols] = (rs2[:, cols].astype(F32) + part[yy(d), :, cols].astype(F32)).astype(BF16)
         there = pl.ds(n * 256, 256)
-        links.put(mg.at[:, there], rs3.at[:, there], q3[n], tp=yy(d))
+        links.put(mg.at[:, there], rs3.at[:, there], g_q3, q3[n], tp=yy(d))
 
     for n in range(NZ):
         cols = slice(n * 256, (n + 1) * 256)
@@ -503,8 +489,8 @@
         for k in range(NY):
             part[k, :, cols] = acc[k * OUT_ROWS : (k + 1) * OUT_ROWS].astype(BF16)
         d = 1 if n % 2 == 0 else -1
-        links.put(part.at[yy(2), :, there], rs2.at[:, there], q2[n], tp=yy(d))
-        links.put(part.at[yy(-d), :, there], rs1.at[:, there], q1[n], tp=yy(-d))
+        links.put(part.at[yy(2), :, there], rs2.at[:, there], g_q2, q2[n], tp=yy(d))
+        links.put(part.at[yy(-d), :, there], rs1.at[:, there], g_q1, q1[n], tp=yy(-d))
         if n >= 2:
             relay(n - 2)
     relay(NZ - 2)
@@ -517,7 +503,7 @@
         links.got(rs3.at[:, there], q3[n], tp=yy(d))
         total = part[y, :, cols].astype(F32) + rs1[:, cols].astype(F32) + rs3[:, cols].astype(F32)
         out[:, cols] = total.astype(BF16)
-    links.drain()
+    links.drain(**after)
 
 
 def per_device(
@@ -565,8 +551,8 @@
             buf((OUT_ROWS, D), BF16),
             buf((OUT_ROWS, D), BF16),
             buf((OUT_ROWS, D), BF16),
-            pltpu.SemaphoreType.DMA((N_DMA,)),
-            pltpu.SemaphoreType.DMA((N_DMA,)),
+            pltpu.SemaphoreType.DMA((N_SEND,)),
+            pltpu.SemaphoreType.DMA((N_RECV,)),
             pltpu.SemaphoreType.DMA((N_LOCAL,)),
         ],
         compiler_params=pltpu.CompilerParams(

time: 82.2 us -> 76.5 us (0.931)
  Pallas kernels: 79.3 us -> 73.9 us
    pallas_call x1, Pallas kernels: 79.3 us -> 73.9 us  [per_device(): pl.pallas_call(layer, out_shape=jax.ShapeDtypeStruct((OUT_ROWS, D), BF16)...]
where the time goes in v3:
time: 76.5 us; the launch traced here: 75.7 us
  Pallas kernels  73.9 us (97%)
  local copies, waits for them, and re-layouts  1.77 us (2%)
    pallas_call x1, Pallas kernels, per_device(): pl.pallas_call(layer, out_shape=jax.ShapeDtypeStruct((OUT_ROWS, D), BF16)...  73.9 us
    unnamed x1, local copies, waits for them, and re-layouts  1.77 us

profile of v3, /device:TPU:8, one launch (start us, length us, event | category | flops | bytes accessed | tf_op | source)
XLA Modules:
  0.0 75.7 jit_solution(15241600154944842941)
XLA Ops:
  0.0 73.9 %layer.1 = bf16[96,2048]{1,0:T(8,128)(2,1)} custom-call(bf16[384,512]{1,0:T(8,128)(2,1)} %tokens.1, f32[1,2048]{1,0:T(1,128)} %bitcast.5, bf16[32,512]{1,0:T(8,128)(2,1)} %wpi.1, bf16[32,512]{1,0:T(8,128)(2,1)} %wli.1, bf16[1,512,512]{2,1,0:T(8,128)(2,1)} %pmix.1, bf16[4,512]{1,0:T(4,128)(2,1)} %taps.1, bf16[2,4,128,128]{3,2,1,0:T(8,128)(2,1)} %rgate.1, ...), custom_call_target="tpu_custom_call" | custom-call | tf_op jit(solution)/shard_map/layer/pallas_call | solution.py:516
  73.9 1.8 %copy.15 = bf16[96,2048]{1,0:T(8,128)(2,1)} copy(bf16[96,2048]{1,0:T(8,128)(2,1)} %layer.1) | data formatting | bytes 786432

commit v4 on v3

--- a/solution.py
+++ b/solution.py
@@ -19,6 +19,7 @@
 CH = 512
 SEGS = 8
 SEG = TOK // SEGS
+STEP = SEG + 1
 OWN = REACH * GRID_W
 EXT = TOK + 2 * OWN
 PAD = 16
@@ -142,20 +143,16 @@
     def at(f, *args):
         return functools.partial(f, *args)
 
-    rounds = [[first, at(b_spread, 0)]]
-    rounds.append(
-        [at(a_side, 1), at(a_side, 3)]
-        + [at(b_hop, s, 1) for s in both]
-        + [at(a_hop, s, 1, 0) for s in both]
-        + [at(a_side, 2)]
-    )
-    for k in (2, 3, 4, 5):
-        turn = [at(b_hop, s, k) for s in both] + [at(a_hop, s, k, 0) for s in both]
-        turn += [at(a_hop, s, k - 1, e) for e in (3, 1, 2) for s in both]
-        turn += [at(row_done, d) for d in ((0,) if k == 2 else (2 - k, k - 2))]
-        rounds.append(turn)
-    rounds.append([at(row_done, 4)])
-    return rounds, arrived
+    along_b = [[at(b_spread, 0)]] + [[at(b_hop, s, k) for s in both] for k in range(1, 5)]
+    along_a = [[first], [at(a_side, 1), at(a_side, 3)]]
+    along_a[1] += [at(a_hop, s, 1, 0) for s in both] + [at(a_side, 2)]
+    for k in range(2, 6):
+        along_a.append(
+            [at(a_hop, s, k, 0) for s in both]
+            + [at(a_hop, s, k - 1, e) for e in (3, 1, 2) for s in both]
+        )
+    rows = [[at(row_done, d) for d in ds] for ds in ((0,), (-1, 1), (-2, 2), (-3, 3), (4,))]
+    return along_a, along_b, rows, arrived
 
 
 def logistic(v):
@@ -259,16 +256,15 @@
             h = i if d == 1 else 1 - i
             piece = tok.at[y, halves[h]]
             links.put(piece, piece, g_t1, t1[d, h], tp=yy(d))
-    r_in, in_arrived = weight_gather(links, win, z, x, c)
-    r_out, out_arrived = weight_gather(links, wout, z, x, c)
+    in_a, in_b, in_rows, in_arrived = weight_gather(links, win, z, x, c)
+    out_a, out_b, out_rows, out_arrived = weight_gather(links, wout, z, x, c)
 
     def serve(*rounds):
         for turn in rounds:
             for step in turn:
                 step()
 
-    serve(r_in[0])
-    serve(r_out[0][:1])
+    serve(in_a[0], in_b[0], out_a[0])
 
     def token_relay():
         for d, h in ((1, 0), (-1, 1)):
@@ -276,14 +272,14 @@
             links.got(piece, t1[d, h], tp=yy(d))
             links.put(piece, piece, g_t2, t2[d], tp=yy(d))
 
-    serve(r_in[1])
-    serve(r_in[2])
+    serve(in_a[1][:2], in_b[1], in_a[1][2:])
+    serve(in_b[2], in_a[2], in_rows[0])
     token_relay()
-    serve(r_out[0][1:])
-    serve(r_in[3])
-    serve(r_in[4])
-    serve(r_out[1])
-    serve(r_in[5], r_in[6])
+    serve(out_b[0])
+    serve(in_b[3], in_a[3], in_rows[1])
+    serve(in_b[4], in_a[4], in_rows[2])
+    serve(out_b[1], out_a[1])
+    serve(in_a[5], in_rows[3], in_rows[4])
     for d, h in ((1, 1), (-1, 0)):
         links.got(tok.at[yy(-d), halves[h]], t1[d, h], tp=yy(d))
     for d, h in ((1, 0), (-1, 1)):
@@ -302,8 +298,9 @@
             nrm[rows, cols] = (v * scale * gain[:, cols]).astype(BF16)
         return 0
 
+    serve(out_b[2])
     lax.fori_loop(0, TOK // 32, norm, 0)
-    serve(r_out[2])
+    serve(out_b[3], out_a[2])
     in_arrived()
 
     def project(col):
@@ -326,7 +323,7 @@
     links.put(pext.at[pl.ds(TOK, OWN)], pext.at[pl.ds(0, OWN)], g_ph, ph[1], **after)
     links.put(pext.at[pl.ds(OWN, OWN)], pext.at[pl.ds(OWN + TOK, OWN)], g_ph, ph[-1], **before)
 
-    serve(r_out[3])
+    serve(out_rows[0])
     links.got(hb.at[0], ch[1], **after)
     links.got(hb.at[1], ch[-1], **before)
     has_before = jnp.where(s > 0, 1.0, 0.0).astype(F32)
@@ -350,8 +347,8 @@
             gs[2 * d] = jnp.dot(conv, rgv[d, b], preferred_element_type=F32)
             gs[2 * d + 1] = jnp.dot(conv, igv[d, b], preferred_element_type=F32)
 
-        def rows_of(i, _):
-            rows = pl.ds(pl.multiple_of(i * 32, 32), 32)
+        for j in range(SEGS):
+            rows, padded = slice(j * SEG, (j + 1) * SEG), slice(j * STEP, j * STEP + SEG)
             value = cvb[rows, :]
             for d in range(2):
                 rate = logistic(gs[2 * d, rows, :])
@@ -359,23 +356,19 @@
                 keep_log = -8.0 * rate * decay[d : d + 1, lanes] + ldb[d, rows, :]
                 keep = jnp.exp(keep_log)
                 rest = one_minus_exp(2.0 * keep_log, keep * keep)
-                aa[d, b, rows, :] = keep
-                bb[d, b, rows, :] = root(rest) * gate * value
-            return 0
-
-        lax.fori_loop(0, TOK // 32, rows_of, 0)
+                aa[d, b, padded, :] = keep
+                bb[d, b, padded, :] = root(rest) * gate * value
 
     block(0)
     block(1)
-    serve(r_out[4][:5])
+    serve(out_b[4], out_a[3])
     block(2)
-    serve(r_out[4][5:])
     block(3)
 
     def scan_step(t, carry):
         new = []
         for d in range(2):
-            at = pl.ds(t if d == 0 else SEG - 1 - t, SEGS, stride=SEG)
+            at = pl.ds(t if d == 0 else SEG - 1 - t, SEGS, stride=STEP)
             for b in range(4):
                 prod, state = carry[2 * (4 * d + b)], carry[2 * (4 * d + b) + 1]
                 keep = aa[d, b, at, :]
@@ -407,7 +400,6 @@
     for dx, dc in around:
         links.put(c1.at[me], c1.at[me], g_k1, k1, sp_1=xx(dx), sp_2=lax.rem(c + dc, NC))
 
-    serve(r_out[5], r_out[6])
     loads[3].wait()
     links.got(pext.at[pl.ds(0, OWN)], ph[1], **after)
     links.got(pext.at[pl.ds(OWN + TOK, OWN)], ph[-1], **before)
@@ -439,6 +431,7 @@
     for n in range(2):
         pooled(n)
 
+    serve(out_rows[1], out_a[4])
     links.got(c1.at[pl.ds(0, 7)], k1, **after)
     full, near = combine(c1, me)
     for d in range(2):
@@ -452,6 +445,7 @@
         cols = slice(n * 256, (n + 1) * 256)
         ycat[:, cols] = jnp.dot(pdf[...], pmv[0, :, cols], preferred_element_type=F32).astype(BF16)
 
+    serve(out_rows[2], out_a[5], out_rows[3], out_rows[4])
     links.got(c2.at[pl.ds(0, 7)], k2, **after)
     _, far = combine(c2, z)
     for d in range(2):
@@ -459,11 +453,11 @@
         enter = np_ * fs_ + ns_ + (np_ * fp_) * start[d : d + 1, :]
         ex[0, d] = ex[1, d] + ex[0, d] * enter
     for j in range(SEGS):
-        rows = slice(j * SEG, (j + 1) * SEG)
+        rows, padded = slice(j * SEG, (j + 1) * SEG), slice(j * STEP, j * STEP + SEG)
         for b in range(4):
             lanes = slice(b * 128, (b + 1) * 128)
-            h0 = bb[0, b, rows, :] + aa[0, b, rows, :] * ex[0, 0, j : j + 1, lanes]
-            h1 = bb[1, b, rows, :] + aa[1, b, rows, :] * ex[0, 1, j : j + 1, lanes]
+            h0 = bb[0, b, padded, :] + aa[0, b, padded, :] * ex[0, 0, j : j + 1, lanes]
+            h1 = bb[1, b, padded, :] + aa[1, b, padded, :] * ex[0, 1, j : j + 1, lanes]
             ycat[rows, CH + b * 128 : CH + (b + 1) * 128] = (h0 + h1).astype(BF16)
     out_arrived()
 
@@ -539,8 +533,8 @@
             buf((EXT, CH), BF16),
             buf((TOK, CH), BF16),
             buf((4, TOK, 128), F32),
-            buf((2, 4, TOK, 128), F32),
-            buf((2, 4, TOK, 128), F32),
+            buf((2, 4, SEGS * STEP, 128), F32),
+            buf((2, 4, SEGS * STEP, 128), F32),
             buf((2, 2, SEGS, CH), F32),
             buf((2, 2, SEGS, CH), F32),
             buf((NX * NC, 4, CH), F32),

time: 76.5 us -> 73.1 us (0.956)
  Pallas kernels: 73.9 us -> 70.4 us
    pallas_call x1, Pallas kernels: 73.9 us -> 70.4 us  [per_device(): pl.pallas_call(layer, out_shape=jax.ShapeDtypeStruct((OUT_ROWS, D), BF16)...]
where the time goes in v4:
time: 73.1 us; the launch traced here: 72.2 us
  Pallas kernels  70.4 us (96%)
  local copies, waits for them, and re-layouts  1.77 us (2%)
    pallas_call x1, Pallas kernels, per_device(): pl.pallas_call(layer, out_shape=jax.ShapeDtypeStruct((OUT_ROWS, D), BF16)...  70.4 us
    unnamed x1, local copies, waits for them, and re-layouts  1.77 us

profile of v4, /device:TPU:8, one launch (start us, length us, event | category | flops | bytes accessed | tf_op | source)
XLA Modules:
  0.0 72.2 jit_solution(15063741449071169669)
XLA Ops:
  0.0 70.4 %layer.1 = bf16[96,2048]{1,0:T(8,128)(2,1)} custom-call(bf16[384,512]{1,0:T(8,128)(2,1)} %tokens.1, f32[1,2048]{1,0:T(1,128)} %bitcast.5, bf16[32,512]{1,0:T(8,128)(2,1)} %wpi.1, bf16[32,512]{1,0:T(8,128)(2,1)} %wli.1, bf16[1,512,512]{2,1,0:T(8,128)(2,1)} %pmix.1, bf16[4,512]{1,0:T(4,128)(2,1)} %taps.1, bf16[2,4,128,128]{3,2,1,0:T(8,128)(2,1)} %rgate.1, ...), custom_call_target="tpu_custom_call" | custom-call | tf_op jit(solution)/shard_map/layer/pallas_call | solution.py:510
  70.4 1.8 %copy.15 = bf16[96,2048]{1,0:T(8,128)(2,1)} copy(bf16[96,2048]{1,0:T(8,128)(2,1)} %layer.1) | data formatting | bytes 786432

commit v5 on v4

--- a/solution.py
+++ b/solution.py
@@ -25,7 +25,7 @@
 PAD = 16
 OUT_ROWS = TOK // NY
 N_SEND = 19
-N_RECV = 130
+N_RECV = 116
 N_LOCAL = 8
 F32 = jnp.float32
 BF16 = jnp.bfloat16
@@ -171,9 +171,9 @@
 
 
 def layer(
-    tokens, gain, wpi, wli, pmix, taps, rgate, igate, decay, logd, start, wop, wol, out,
+    tokens, gain, wpi, wli, pmix, taps, rgate, igate, decay, logd, start, wop, wol, own, rs1, rs3,
     tok, nrm, win, wout, pmv, rgv, igv, ldb, box, rcp, ulb, ulf, hb, cvb, pext, pdf, gs, aa, bb,
-    sg, ex, c1, c2, ycat, part, rs1, rs2, rs3, mg, send, recv, local,
+    sg, ex, c1, c2, ycat, part, rs2, mg, send, recv, local,
 ):
     z, x, c = (lax.axis_index(n) for n in SP)
     y = lax.axis_index("tp")
@@ -300,7 +300,6 @@
 
     serve(out_b[2])
     lax.fori_loop(0, TOK // 32, norm, 0)
-    serve(out_b[3], out_a[2])
     in_arrived()
 
     def project(col):
@@ -316,6 +315,7 @@
     ch = {d: links.slot() for d in (1, -1)}
     links.put(ulb.at[pl.ds(TOK - PAD, PAD)], hb.at[0], g_ch, ch[1], **after)
     links.put(ulb.at[pl.ds(0, PAD)], hb.at[1], g_ch, ch[-1], **before)
+    serve(out_b[3], out_a[2])
     for n in range(2):
         pext[OWN : OWN + TOK, n * 256 : (n + 1) * 256] = project(n * 256)
     g_ph = links.group(pext.at[pl.ds(0, 2 * OWN)])
@@ -462,9 +462,8 @@
     out_arrived()
 
     g_q1, g_q2, g_q3 = links.group(rs1), links.group(rs2), links.group(rs3)
-    q1 = [links.slot() for _ in range(NZ)]
+    q1, q3 = links.slot(), links.slot()
     q2 = [links.slot() for _ in range(NZ)]
-    q3 = [links.slot() for _ in range(NZ)]
 
     def relay(n):
         cols = slice(n * 256, (n + 1) * 256)
@@ -473,7 +472,7 @@
         links.got(at, q2[n], tp=yy(d))
         mg[:, cols] = (rs2[:, cols].astype(F32) + part[yy(d), :, cols].astype(F32)).astype(BF16)
         there = pl.ds(n * 256, 256)
-        links.put(mg.at[:, there], rs3.at[:, there], g_q3, q3[n], tp=yy(d))
+        links.put(mg.at[:, there], rs3.at[:, there], g_q3, q3, tp=yy(d))
 
     for n in range(NZ):
         cols = slice(n * 256, (n + 1) * 256)
@@ -484,19 +483,16 @@
             part[k, :, cols] = acc[k * OUT_ROWS : (k + 1) * OUT_ROWS].astype(BF16)
         d = 1 if n % 2 == 0 else -1
         links.put(part.at[yy(2), :, there], rs2.at[:, there], g_q2, q2[n], tp=yy(d))
-        links.put(part.at[yy(-d), :, there], rs1.at[:, there], g_q1, q1[n], tp=yy(-d))
-        if n >= 2:
-            relay(n - 2)
-    relay(NZ - 2)
-    relay(NZ - 1)
-    for n in range(NZ):
-        cols = slice(n * 256, (n + 1) * 256)
-        there = pl.ds(n * 256, 256)
-        d = 1 if n % 2 == 0 else -1
-        links.got(rs1.at[:, there], q1[n], tp=yy(-d))
-        links.got(rs3.at[:, there], q3[n], tp=yy(d))
-        total = part[y, :, cols].astype(F32) + rs1[:, cols].astype(F32) + rs3[:, cols].astype(F32)
-        out[:, cols] = total.astype(BF16)
+        links.put(part.at[yy(-d), :, there], rs1.at[:, there], g_q1, q1, tp=yy(-d))
+        if n >= 5:
+            relay(n - 5)
+    keep_own = pltpu.make_async_copy(part.at[y], own, local.at[0])
+    keep_own.start()
+    for n in range(3, NZ):
+        relay(n)
+    links.got(rs1, q1, **after)
+    links.got(rs3, q3, **after)
+    keep_own.wait()
     links.drain(**after)
 
 
@@ -507,14 +503,14 @@
     anywhere = pl.BlockSpec(memory_space=pl.ANY)
     near = pl.BlockSpec(memory_space=pltpu.VMEM)
     buf = pltpu.VMEM
-    return pl.pallas_call(
+    own, near_sum, far_sum = pl.pallas_call(
         layer,
-        out_shape=jax.ShapeDtypeStruct((OUT_ROWS, D), BF16),
+        out_shape=[jax.ShapeDtypeStruct((OUT_ROWS, D), BF16)] * 3,
         in_specs=[
             anywhere, near, anywhere, anywhere, anywhere, near, anywhere, anywhere, near, near,
             near, anywhere, anywhere,
         ],
-        out_specs=near,
+        out_specs=[anywhere] * 3,
         scratch_shapes=[
             buf((NY, TOK, CH), BF16),
             buf((TOK, D), BF16),
@@ -543,8 +539,6 @@
             buf((NY, OUT_ROWS, D), BF16),
             buf((OUT_ROWS, D), BF16),
             buf((OUT_ROWS, D), BF16),
-            buf((OUT_ROWS, D), BF16),
-            buf((OUT_ROWS, D), BF16),
             pltpu.SemaphoreType.DMA((N_SEND,)),
             pltpu.SemaphoreType.DMA((N_RECV,)),
             pltpu.SemaphoreType.DMA((N_LOCAL,)),
@@ -557,6 +551,8 @@
         tokens, norm_gain.reshape(1, D), w_pool_in, w_lru_in, pool_mix, conv_taps, rec_gate,
         in_gate, decay_rate, log_decay, start_state, w_out_pool.T, w_out_lru.T,
     )
+    total = own.astype(F32) + near_sum.astype(F32) + far_sum.astype(F32)
+    return total.astype(BF16)
 
 
 def solution(mesh):

time: 73.1 us -> 71.6 us (0.979)
  other arithmetic: 0 us -> 2.13 us
  Pallas kernels: 70.4 us -> 68.5 us
  local copies, waits for them, and re-layouts: 1.77 us -> 0 us
    convert_element_type x0 -> x1, other arithmetic: none -> 2.13 us  [per_device(): return total.astype(BF16)]
    pallas_call x1, Pallas kernels: 70.4 us -> 68.5 us  [per_device(): pl.pallas_call(layer, out_shape=[jax.ShapeDtypeStruct((OUT_ROWS, D), BF16...]
    unnamed x1 -> x0, local copies, waits for them, and re-layouts: 1.77 us -> none
where the time goes in v5:
time: 71.6 us; the launch traced here: 70.7 us
  Pallas kernels  68.5 us (96%)
  other arithmetic  2.13 us (3%)
    pallas_call x1, Pallas kernels, per_device(): pl.pallas_call(layer, out_shape=[jax.ShapeDtypeStruct((OUT_ROWS, D), BF16...  68.5 us
    convert_element_type x1, other arithmetic, per_device(): return total.astype(BF16)  2.13 us

profile of v5, /device:TPU:8, one launch (start us, length us, event | category | flops | bytes accessed | tf_op | source)
XLA Modules:
  0.0 70.7 jit_solution(5940486183926005441)
XLA Ops:
  0.0 68.5 %layer.1 = (bf16[96,2048]{1,0:T(8,128)(2,1)}, bf16[96,2048]{1,0:T(8,128)(2,1)}, bf16[96,2048]{1,0:T(8,128)(2,1)}) custom-call(bf16[384,512]{1,0:T(8,128)(2,1)} %tokens.1, f32[1,2048]{1,0:T(1,128)} %bitcast.5, bf16[32,512]{1,0:T(8,128)(2,1)} %wpi.1, bf16[32,512]{1,0:T(8,128)(2,1)} %wli.1, bf16[1,512,512]{2,1,0:T(8,128)(2,1)} %pmix.1, bf16[4,512]{1,0:T(4,128)(2,1)} %taps.1, ...), custom_call_target="tpu_custom_call" | custom-call | tf_op jit(solution)/shard_map/layer/pallas_call | solution.py:506
  68.5 2.1 %add_convert_fusion = bf16[96,2048]{1,0:T(8,128)(2,1)} fusion(bf16[96,2048]{1,0:T(8,128)(2,1)} %get-tuple-element.10, bf16[96,2048]{1,0:T(8,128)(2,1)} %get-tuple-element.9, bf16[96,2048]{1,0:T(8,128)(2,1)} %get-tuple-element.8), kind=kLoop, calls=%fused_computation | loop fusion | flops 1179648 | bytes 1572864 | tf_op jit(solution)/shard_map/convert_element_type | solution.py:555

commit v6 on v5

--- a/solution.py
+++ b/solution.py
@@ -25,7 +25,7 @@
 PAD = 16
 OUT_ROWS = TOK // NY
 N_SEND = 19
-N_RECV = 116
+N_RECV = 123
 N_LOCAL = 8
 F32 = jnp.float32
 BF16 = jnp.bfloat16
@@ -65,7 +65,7 @@
             self.copy(region, region, group, 0, dev).wait_send()
 
 
-def weight_gather(links, buf, z, x, c):
+def weight_gather(links, buf, z, x, c, by_row):
     lo, hi = pl.ds(0, 16), pl.ds(16, 16)
 
     def zz(d):
@@ -86,7 +86,7 @@
     }
     b1 = {(s, k): links.slot() for s in both for k in range(1, 5 if s == 1 else 4)}
     b2 = {d: links.slot() for d in rel}
-    dd = links.slot()
+    dd = {d: links.slot() for d in rel} if by_row else dict.fromkeys(rel, links.slot())
     g_a1 = links.group(buf.at[0, pl.ds(0, 3), c, lo])
     g_a2 = links.group(buf.at[pl.ds(0, 7), pl.ds(0, NX), c, lo])
     g_b1 = links.group(buf.at[pl.ds(0, 7), 0, c, lo])
@@ -127,7 +127,7 @@
     def row_done(d):
         links.got(buf.at[zz(d), pl.ds(0, 3), c, hi], b2[d], sp_1=xx(1))
         row = buf.at[zz(d), pl.ds(0, NX), c]
-        links.put(row, row, g_dd, dd, **other)
+        links.put(row, row, g_dd, dd[d], **other)
 
     def first():
         own = buf.at[z, x, c, lo]
@@ -137,8 +137,9 @@
             b_send(s, 1)
             a_send(s, 1, 0)
 
-    def arrived():
-        links.got(buf.at[pl.ds(0, NZ), pl.ds(0, NX), 1 - c], dd, **other)
+    def arrived(d):
+        of = zz(d) if by_row else pl.ds(0, NZ)
+        links.got(buf.at[of, pl.ds(0, NX), 1 - c], dd[d], **other)
 
     def at(f, *args):
         return functools.partial(f, *args)
@@ -256,8 +257,8 @@
             h = i if d == 1 else 1 - i
             piece = tok.at[y, halves[h]]
             links.put(piece, piece, g_t1, t1[d, h], tp=yy(d))
-    in_a, in_b, in_rows, in_arrived = weight_gather(links, win, z, x, c)
-    out_a, out_b, out_rows, out_arrived = weight_gather(links, wout, z, x, c)
+    in_a, in_b, in_rows, in_arrived = weight_gather(links, win, z, x, c, False)
+    out_a, out_b, out_rows, out_arrived = weight_gather(links, wout, z, x, c, True)
 
     def serve(*rounds):
         for turn in rounds:
@@ -300,7 +301,7 @@
 
     serve(out_b[2])
     lax.fori_loop(0, TOK // 32, norm, 0)
-    in_arrived()
+    in_arrived(0)
 
     def project(col):
         w = win[:, :, :, :, col : col + 256].reshape(D, 256)
@@ -361,7 +362,6 @@
 
     block(0)
     block(1)
-    serve(out_b[4], out_a[3])
     block(2)
     block(3)
 
@@ -400,9 +400,7 @@
     for dx, dc in around:
         links.put(c1.at[me], c1.at[me], g_k1, k1, sp_1=xx(dx), sp_2=lax.rem(c + dc, NC))
 
-    loads[3].wait()
-    links.got(pext.at[pl.ds(0, OWN)], ph[1], **after)
-    links.got(pext.at[pl.ds(OWN + TOK, OWN)], ph[-1], **before)
+    serve(out_b[4], out_a[3])
 
     def combine(table, mine):
         full, inside = [], []
@@ -428,10 +426,6 @@
         scale = jnp.concatenate([rcp[...], rcp[...]], axis=1)
         pdf[:, cols] = (total * scale - own).astype(BF16)
 
-    for n in range(2):
-        pooled(n)
-
-    serve(out_rows[1], out_a[4])
     links.got(c1.at[pl.ds(0, 7)], k1, **after)
     full, near = combine(c1, me)
     for d in range(2):
@@ -441,11 +435,17 @@
     for d in range(1, NZ):
         links.put(c2.at[z], c2.at[z], g_k2, k2, sp_0=zz(d))
 
+    serve(out_rows[1], out_rows[2], out_a[4])
+    loads[3].wait()
+    links.got(pext.at[pl.ds(0, OWN)], ph[1], **after)
+    links.got(pext.at[pl.ds(OWN + TOK, OWN)], ph[-1], **before)
+    for n in range(2):
+        pooled(n)
     for n in range(2):
         cols = slice(n * 256, (n + 1) * 256)
         ycat[:, cols] = jnp.dot(pdf[...], pmv[0, :, cols], preferred_element_type=F32).astype(BF16)
 
-    serve(out_rows[2], out_a[5], out_rows[3], out_rows[4])
+    serve(out_rows[3])
     links.got(c2.at[pl.ds(0, 7)], k2, **after)
     _, far = combine(c2, z)
     for d in range(2):
@@ -459,11 +459,13 @@
             h0 = bb[0, b, padded, :] + aa[0, b, padded, :] * ex[0, 0, j : j + 1, lanes]
             h1 = bb[1, b, padded, :] + aa[1, b, padded, :] * ex[0, 1, j : j + 1, lanes]
             ycat[rows, CH + b * 128 : CH + (b + 1) * 128] = (h0 + h1).astype(BF16)
-    out_arrived()
-
     g_q1, g_q2, g_q3 = links.group(rs1), links.group(rs2), links.group(rs3)
     q1, q3 = links.slot(), links.slot()
     q2 = [links.slot() for _ in range(NZ)]
+
+    def tile(n):
+        turn = (0, -1, 1, -2, 2, -3, 3, 4)[n]
+        return pl.ds(pl.multiple_of(zz(turn) * 256, 256), 256)
 
     def relay(n):
         cols = slice(n * 256, (n + 1) * 256)
@@ -472,27 +474,29 @@
         links.got(at, q2[n], tp=yy(d))
         mg[:, cols] = (rs2[:, cols].astype(F32) + part[yy(d), :, cols].astype(F32)).astype(BF16)
         there = pl.ds(n * 256, 256)
-        links.put(mg.at[:, there], rs3.at[:, there], g_q3, q3, tp=yy(d))
-
-    for n in range(NZ):
+        links.put(mg.at[:, there], rs3.at[:, tile(n)], g_q3, q3, tp=yy(d))
+
+    for n, turn in enumerate((0, -1, 1, -2, 2, -3, 3, 4)):
         cols = slice(n * 256, (n + 1) * 256)
-        there = pl.ds(n * 256, 256)
-        w = wout[n].reshape(256, 2 * CH)
+        here = pl.ds(n * 256, 256)
+        out_arrived(turn)
+        w = wout[zz(turn)].reshape(256, 2 * CH)
         acc = lax.dot_general(ycat[...], w, NT, preferred_element_type=F32)
         for k in range(NY):
             part[k, :, cols] = acc[k * OUT_ROWS : (k + 1) * OUT_ROWS].astype(BF16)
         d = 1 if n % 2 == 0 else -1
-        links.put(part.at[yy(2), :, there], rs2.at[:, there], g_q2, q2[n], tp=yy(d))
-        links.put(part.at[yy(-d), :, there], rs1.at[:, there], g_q1, q1, tp=yy(-d))
+        links.put(part.at[yy(2), :, here], rs2.at[:, here], g_q2, q2[n], tp=yy(d))
+        links.put(part.at[yy(-d), :, here], rs1.at[:, tile(n)], g_q1, q1, tp=yy(-d))
+        pltpu.make_async_copy(part.at[y, :, here], own.at[:, tile(n)], local.at[0]).start()
+        if n == 2:
+            serve(out_a[5], out_rows[4])
         if n >= 5:
             relay(n - 5)
-    keep_own = pltpu.make_async_copy(part.at[y], own, local.at[0])
-    keep_own.start()
     for n in range(3, NZ):
         relay(n)
     links.got(rs1, q1, **after)
     links.got(rs3, q3, **after)
-    keep_own.wait()
+    pltpu.make_async_copy(rs1, own, local.at[0]).wait()
     links.drain(**after)
 
 

time: 71.6 us -> 69.8 us (0.975); the launches traced: 70.7 us -> 69.6 us
  Pallas kernels: 68.5 us -> 67.5 us
    pallas_call x1, Pallas kernels: 68.5 us -> 67.5 us  [per_device(): pl.pallas_call(layer, out_shape=[jax.ShapeDtypeStruct((OUT_ROWS, D), BF16...]
where the time goes in v6:
time: 69.8 us; the launch traced here: 69.6 us
  Pallas kernels  67.5 us (97%)
  other arithmetic  2.13 us (3%)
    pallas_call x1, Pallas kernels, per_device(): pl.pallas_call(layer, out_shape=[jax.ShapeDtypeStruct((OUT_ROWS, D), BF16...  67.5 us
    convert_element_type x1, other arithmetic, per_device(): return total.astype(BF16)  2.13 us

profile of v6, /device:TPU:8, one launch (start us, length us, event | category | flops | bytes accessed | tf_op | source)
XLA Modules:
  0.0 69.6 jit_solution(13679374979972317288)
XLA Ops:
  0.0 67.5 %layer.1 = (bf16[96,2048]{1,0:T(8,128)(2,1)}, bf16[96,2048]{1,0:T(8,128)(2,1)}, bf16[96,2048]{1,0:T(8,128)(2,1)}) custom-call(bf16[384,512]{1,0:T(8,128)(2,1)} %tokens.1, f32[1,2048]{1,0:T(1,128)} %bitcast.5, bf16[32,512]{1,0:T(8,128)(2,1)} %wpi.1, bf16[32,512]{1,0:T(8,128)(2,1)} %wli.1, bf16[1,512,512]{2,1,0:T(8,128)(2,1)} %pmix.1, bf16[4,512]{1,0:T(4,128)(2,1)} %taps.1, ...), custom_call_target="tpu_custom_call" | custom-call | tf_op jit(solution)/shard_map/layer/pallas_call | solution.py:510
  67.5 2.1 %add_convert_fusion = bf16[96,2048]{1,0:T(8,128)(2,1)} fusion(bf16[96,2048]{1,0:T(8,128)(2,1)} %get-tuple-element.10, bf16[96,2048]{1,0:T(8,128)(2,1)} %get-tuple-element.9, bf16[96,2048]{1,0:T(8,128)(2,1)} %get-tuple-element.8), kind=kLoop, calls=%fused_computation | loop fusion | flops 1179648 | bytes 1572864 | tf_op jit(solution)/shard_map/convert_element_type | solution.py:559

commit v7 on v6

--- a/solution.py
+++ b/solution.py
@@ -24,8 +24,8 @@
 EXT = TOK + 2 * OWN
 PAD = 16
 OUT_ROWS = TOK // NY
-N_SEND = 19
-N_RECV = 123
+N_SEND = 20
+N_RECV = 124
 N_LOCAL = 8
 F32 = jnp.float32
 BF16 = jnp.bfloat16
@@ -173,7 +173,7 @@
 
 def layer(
     tokens, gain, wpi, wli, pmix, taps, rgate, igate, decay, logd, start, wop, wol, own, rs1, rs3,
-    tok, nrm, win, wout, pmv, rgv, igv, ldb, box, rcp, ulb, ulf, hb, cvb, pext, pdf, gs, aa, bb,
+    tok, nrm, win, wout, pmv, rgv, igv, ldb, box, rcp, ulf, hal, cvb, pext, pdf, gs, aa, bb,
     sg, ex, c1, c2, ycat, part, rs2, mg, send, recv, local,
 ):
     z, x, c = (lax.axis_index(n) for n in SP)
@@ -210,7 +210,7 @@
         load.start()
 
     barrier = pltpu.get_barrier_semaphore()
-    peers = [{"tp": yy(1)}, {"tp": yy(-1)}, after, before]
+    peers = [{"tp": yy(1)}, {"tp": yy(-1)}, {"tp": yy(2)}, after, before]
     peers += [{"sp_0": zz(d)} for d in range(1, NZ)]
     around = [(dx, dc) for dx in range(NX) for dc in range(NC) if dx or dc]
     for dx, dc in around:
@@ -257,6 +257,10 @@
             h = i if d == 1 else 1 - i
             piece = tok.at[y, halves[h]]
             links.put(piece, piece, g_t1, t1[d, h], tp=yy(d))
+    g_ch, g_hs = links.group(hal.at[0]), links.group(hal.at[pl.ds(0, 3)])
+    ch, hs = {d: links.slot() for d in (1, -1)}, links.slot()
+    links.put(tok.at[y, pl.ds(TOK - PAD, PAD)], hal.at[y, 0], g_ch, ch[1], **after)
+    links.put(tok.at[y, pl.ds(0, PAD)], hal.at[y, 1], g_ch, ch[-1], **before)
     in_a, in_b, in_rows, in_arrived = weight_gather(links, win, z, x, c, False)
     out_a, out_b, out_rows, out_arrived = weight_gather(links, wout, z, x, c, True)
 
@@ -274,6 +278,10 @@
             links.put(piece, piece, g_t2, t2[d], tp=yy(d))
 
     serve(in_a[1][:2], in_b[1], in_a[1][2:])
+    links.got(hal.at[y, 0], ch[1], **after)
+    links.got(hal.at[y, 1], ch[-1], **before)
+    for d in (1, -1, 2):
+        links.put(hal.at[y], hal.at[y], g_hs, hs, tp=yy(d))
     serve(in_b[2], in_a[2], in_rows[0])
     token_relay()
     serve(out_b[0])
@@ -286,53 +294,45 @@
     for d, h in ((1, 0), (-1, 1)):
         links.got(tok.at[yy(2), halves[h]], t2[d], tp=yy(d))
 
-    def norm(i, _):
-        rows = pl.ds(pl.multiple_of(i * 32, 32), 32)
+    links.got(hal.at[pl.ds(0, 3)], hs, tp=yy(1))
+
+    def normed(parts, rows):
         total = jnp.zeros((32, 1), F32)
         for k in range(NY):
-            v = tok[k, rows, :].astype(F32)
+            v = parts(k).astype(F32)
             total = total + jnp.sum(v * v, axis=1, keepdims=True)
         scale = lax.rsqrt(total * (1.0 / D) + EPS)
         for k in range(NY):
             cols = slice(k * CH, (k + 1) * CH)
-            v = tok[k, rows, :].astype(F32)
+            v = parts(k).astype(F32)
             nrm[rows, cols] = (v * scale * gain[:, cols]).astype(BF16)
+
+    def norm(i, _):
+        rows = pl.ds(pl.multiple_of(i * 32, 32), 32)
+        normed(lambda k: tok[k, rows, :], rows)
         return 0
 
     serve(out_b[2])
     lax.fori_loop(0, TOK // 32, norm, 0)
+    normed(lambda k: hal[k].reshape(2 * PAD, CH), pl.ds(TOK, 2 * PAD))
     in_arrived(0)
 
-    def project(col):
-        w = win[:, :, :, :, col : col + 256].reshape(D, 256)
-        return jnp.dot(nrm[...], w, preferred_element_type=F32).astype(BF16)
-
-    for n in range(2):
-        u = project(CH + n * 256)
-        ulb[:, n * 256 : (n + 1) * 256] = u
-        for k in range(2):
-            ulf[2 * n + k, PAD : PAD + TOK, :] = u[:, k * 128 : (k + 1) * 128].astype(F32)
-    g_ch = links.group(hb)
-    ch = {d: links.slot() for d in (1, -1)}
-    links.put(ulb.at[pl.ds(TOK - PAD, PAD)], hb.at[0], g_ch, ch[1], **after)
-    links.put(ulb.at[pl.ds(0, PAD)], hb.at[1], g_ch, ch[-1], **before)
-    serve(out_b[3], out_a[2])
-    for n in range(2):
-        pext[OWN : OWN + TOK, n * 256 : (n + 1) * 256] = project(n * 256)
-    g_ph = links.group(pext.at[pl.ds(0, 2 * OWN)])
-    ph = {d: links.slot() for d in (1, -1)}
-    links.put(pext.at[pl.ds(TOK, OWN)], pext.at[pl.ds(0, OWN)], g_ph, ph[1], **after)
-    links.put(pext.at[pl.ds(OWN, OWN)], pext.at[pl.ds(OWN + TOK, OWN)], g_ph, ph[-1], **before)
-
-    serve(out_rows[0])
-    links.got(hb.at[0], ch[1], **after)
-    links.got(hb.at[1], ch[-1], **before)
     has_before = jnp.where(s > 0, 1.0, 0.0).astype(F32)
     has_after = jnp.where(s < NZ * NX * NC - 1, 1.0, 0.0).astype(F32)
-    for b in range(4):
-        lanes = slice(b * 128, (b + 1) * 128)
-        ulf[b, 0:PAD, :] = hb[0, :, lanes].astype(F32) * has_before
-        ulf[b, PAD + TOK :, :] = hb[1, :, lanes].astype(F32) * has_after
+
+    def project(col, rows):
+        w = win[:, :, :, :, col : col + 256].reshape(D, 256)
+        return jnp.dot(nrm[:rows, :], w, preferred_element_type=F32).astype(BF16)
+
+    for n in range(2):
+        u = project(CH + n * 256, TOK + 2 * PAD)
+        for k in range(2):
+            v = u[:, k * 128 : (k + 1) * 128].astype(F32)
+            ulf[2 * n + k, PAD : PAD + TOK, :] = v[:TOK]
+            ulf[2 * n + k, 0:PAD, :] = v[TOK : TOK + PAD] * has_before
+            ulf[2 * n + k, PAD + TOK :, :] = v[TOK + PAD :] * has_after
+    serve(out_b[3], out_a[2])
+    serve(out_rows[0])
     for load in loads[4:6]:
         load.wait()
 
@@ -400,6 +400,12 @@
     for dx, dc in around:
         links.put(c1.at[me], c1.at[me], g_k1, k1, sp_1=xx(dx), sp_2=lax.rem(c + dc, NC))
 
+    for n in range(2):
+        pext[OWN : OWN + TOK, n * 256 : (n + 1) * 256] = project(n * 256, TOK)
+    g_ph = links.group(pext.at[pl.ds(0, 2 * OWN)])
+    ph = {d: links.slot() for d in (1, -1)}
+    links.put(pext.at[pl.ds(TOK, OWN)], pext.at[pl.ds(0, OWN)], g_ph, ph[1], **after)
+    links.put(pext.at[pl.ds(OWN, OWN)], pext.at[pl.ds(OWN + TOK, OWN)], g_ph, ph[-1], **before)
     serve(out_b[4], out_a[3])
 
     def combine(table, mine):
@@ -517,7 +523,7 @@
         out_specs=[anywhere] * 3,
         scratch_shapes=[
             buf((NY, TOK, CH), BF16),
-            buf((TOK, D), BF16),
+            buf((TOK + 2 * PAD, D), BF16),
             buf((NZ, NX, NC, 32, 2 * CH), BF16),
             buf((NZ, NX, NC, 32, 2 * CH), BF16),
             buf((1, CH, CH), BF16),
@@ -526,15 +532,14 @@
             buf((2, TOK, 128), F32),
             buf((TOK, EXT), BF16),
             buf((TOK, 128), F32),
-            buf((TOK, CH), BF16),
             buf((4, TOK + 2 * PAD, 128), F32),
-            buf((2, PAD, CH), BF16),
+            buf((NY, 2, PAD, CH), BF16),
             buf((TOK, 128), F32),
             buf((EXT, CH), BF16),
             buf((TOK, CH), BF16),
             buf((4, TOK, 128), F32),
-            buf((2, 4, SEGS * STEP, 128), F32),
-            buf((2, 4, SEGS * STEP, 128), F32),
+            buf((2, 4, SEGS * STEP + SEG, 128), F32),
+            buf((2, 4, SEGS * STEP + SEG, 128), F32),
             buf((2, 2, SEGS, CH), F32),
             buf((2, 2, SEGS, CH), F32),
             buf((NX * NC, 4, CH), F32),

time: 69.8 us -> 68.3 us (0.979)
  Pallas kernels: 67.5 us -> 66 us
    pallas_call x1, Pallas kernels: 67.5 us -> 66 us  [per_device(): pl.pallas_call(layer, out_shape=[jax.ShapeDtypeStruct((OUT_ROWS, D), BF16...]
where the time goes in v7:
time: 68.3 us; the launch traced here: 68.2 us
  Pallas kernels  66 us (97%)
  other arithmetic  2.13 us (3%)
    pallas_call x1, Pallas kernels, per_device(): pl.pallas_call(layer, out_shape=[jax.ShapeDtypeStruct((OUT_ROWS, D), BF16...  66 us
    convert_element_type x1, other arithmetic, per_device(): return total.astype(BF16)  2.13 us

profile of v7, /device:TPU:8, one launch (start us, length us, event | category | flops | bytes accessed | tf_op | source)
XLA Modules:
  0.0 68.2 jit_solution(9237795039052253713)
XLA Ops:
  0.0 66.0 %layer.1 = (bf16[96,2048]{1,0:T(8,128)(2,1)}, bf16[96,2048]{1,0:T(8,128)(2,1)}, bf16[96,2048]{1,0:T(8,128)(2,1)}) custom-call(bf16[384,512]{1,0:T(8,128)(2,1)} %tokens.1, f32[1,2048]{1,0:T(1,128)} %bitcast.5, bf16[32,512]{1,0:T(8,128)(2,1)} %wpi.1, bf16[32,512]{1,0:T(8,128)(2,1)} %wli.1, bf16[1,512,512]{2,1,0:T(8,128)(2,1)} %pmix.1, bf16[4,512]{1,0:T(4,128)(2,1)} %taps.1, ...), custom_call_target="tpu_custom_call" | custom-call | tf_op jit(solution)/shard_map/layer/pallas_call | solution.py:516
  66.1 2.1 %add_convert_fusion = bf16[96,2048]{1,0:T(8,128)(2,1)} fusion(bf16[96,2048]{1,0:T(8,128)(2,1)} %get-tuple-element.10, bf16[96,2048]{1,0:T(8,128)(2,1)} %get-tuple-element.9, bf16[96,2048]{1,0:T(8,128)(2,1)} %get-tuple-element.8), kind=kLoop, calls=%fused_computation | loop fusion | flops 1179648 | bytes 1572864 | tf_op jit(solution)/shard_map/convert_element_type | solution.py:564

commit v8 on v7

--- a/solution.py
+++ b/solution.py
@@ -24,8 +24,8 @@
 EXT = TOK + 2 * OWN
 PAD = 16
 OUT_ROWS = TOK // NY
-N_SEND = 20
-N_RECV = 124
+N_SEND = 25
+N_RECV = 171
 N_LOCAL = 8
 F32 = jnp.float32
 BF16 = jnp.bfloat16
@@ -122,7 +122,8 @@
         if (s, k) in b1:
             links.got(buf.at[zz(-s * k), x, c, hi], b1[s, k], sp_0=zz(s))
             b_send(s, k + 1)
-            b_spread(-s * k if k < 4 else 4)
+            if not by_row:
+                b_spread(-s * k if k < 4 else 4)
 
     def row_done(d):
         links.got(buf.at[zz(d), pl.ds(0, 3), c, hi], b2[d], sp_1=xx(1))
@@ -153,7 +154,8 @@
             + [at(a_hop, s, k - 1, e) for e in (3, 1, 2) for s in both]
         )
     rows = [[at(row_done, d) for d in ds] for ds in ((0,), (-1, 1), (-2, 2), (-3, 3), (4,))]
-    return along_a, along_b, rows, arrived
+    spread = [[at(b_spread, d) for d in ds] for ds in ((0,), (-1, 1), (-2, 2), (-3, 3), (4,))]
+    return along_a, along_b, rows, arrived, spread
 
 
 def logistic(v):
@@ -173,7 +175,7 @@
 
 def layer(
     tokens, gain, wpi, wli, pmix, taps, rgate, igate, decay, logd, start, wop, wol, own, rs1, rs3,
-    tok, nrm, win, wout, pmv, rgv, igv, ldb, box, rcp, ulf, hal, cvb, pext, pdf, gs, aa, bb,
+    tok, nrm, wl, wp, wout, pmv, rgv, igv, ldb, box, rcp, ulf, hal, cvb, pext, pdf, gs, aa, bb,
     sg, ex, c1, c2, ycat, part, rs2, mg, send, recv, local,
 ):
     z, x, c = (lax.axis_index(n) for n in SP)
@@ -198,8 +200,8 @@
 
     loads = [
         pltpu.make_async_copy(tokens, tok.at[y], local.at[0]),
-        pltpu.make_async_copy(wpi, win.at[z, x, c, :, pl.ds(0, CH)], local.at[1]),
-        pltpu.make_async_copy(wli, win.at[z, x, c, :, pl.ds(CH, CH)], local.at[2]),
+        pltpu.make_async_copy(wpi, wp.at[z, x, c], local.at[1]),
+        pltpu.make_async_copy(wli, wl.at[z, x, c], local.at[2]),
         pltpu.make_async_copy(pmix, pmv, local.at[3]),
         pltpu.make_async_copy(rgate, rgv, local.at[4]),
         pltpu.make_async_copy(igate, igv, local.at[5]),
@@ -261,15 +263,16 @@
     ch, hs = {d: links.slot() for d in (1, -1)}, links.slot()
     links.put(tok.at[y, pl.ds(TOK - PAD, PAD)], hal.at[y, 0], g_ch, ch[1], **after)
     links.put(tok.at[y, pl.ds(0, PAD)], hal.at[y, 1], g_ch, ch[-1], **before)
-    in_a, in_b, in_rows, in_arrived = weight_gather(links, win, z, x, c, False)
-    out_a, out_b, out_rows, out_arrived = weight_gather(links, wout, z, x, c, True)
+    lru_a, lru_b, lru_rows, lru_arrived, _ = weight_gather(links, wl, z, x, c, False)
+    pool_a, pool_b, pool_rows, pool_arrived, _ = weight_gather(links, wp, z, x, c, False)
+    out_a, out_b, out_rows, out_arrived, out_x = weight_gather(links, wout, z, x, c, True)
 
     def serve(*rounds):
         for turn in rounds:
             for step in turn:
                 step()
 
-    serve(in_a[0], in_b[0], out_a[0])
+    serve(lru_a[0], lru_b[0], pool_a[0])
 
     def token_relay():
         for d, h in ((1, 0), (-1, 1)):
@@ -277,18 +280,18 @@
             links.got(piece, t1[d, h], tp=yy(d))
             links.put(piece, piece, g_t2, t2[d], tp=yy(d))
 
-    serve(in_a[1][:2], in_b[1], in_a[1][2:])
+    serve(lru_a[1][:2], lru_b[1], lru_a[1][2:], pool_b[0])
     links.got(hal.at[y, 0], ch[1], **after)
     links.got(hal.at[y, 1], ch[-1], **before)
     for d in (1, -1, 2):
         links.put(hal.at[y], hal.at[y], g_hs, hs, tp=yy(d))
-    serve(in_b[2], in_a[2], in_rows[0])
+    serve(lru_b[2], lru_a[2], lru_rows[0], pool_b[1], pool_a[1])
     token_relay()
-    serve(out_b[0])
-    serve(in_b[3], in_a[3], in_rows[1])
-    serve(in_b[4], in_a[4], in_rows[2])
-    serve(out_b[1], out_a[1])
-    serve(in_a[5], in_rows[3], in_rows[4])
+    serve(lru_b[3], lru_a[3], lru_rows[1])
+    serve(out_a[0], pool_b[2], pool_a[2], pool_rows[0])
+    serve(lru_b[4], lru_a[4], lru_rows[2])
+    serve(pool_b[3], pool_a[3], pool_rows[1])
+    serve(lru_a[5], lru_rows[3], lru_rows[4], out_b[0])
     for d, h in ((1, 1), (-1, 0)):
         links.got(tok.at[yy(-d), halves[h]], t1[d, h], tp=yy(d))
     for d, h in ((1, 0), (-1, 1)):
@@ -312,27 +315,26 @@
         normed(lambda k: tok[k, rows, :], rows)
         return 0
 
-    serve(out_b[2])
     lax.fori_loop(0, TOK // 32, norm, 0)
     normed(lambda k: hal[k].reshape(2 * PAD, CH), pl.ds(TOK, 2 * PAD))
-    in_arrived(0)
+    serve(pool_b[4], pool_a[4], pool_rows[2])
+    lru_arrived(0)
 
     has_before = jnp.where(s > 0, 1.0, 0.0).astype(F32)
     has_after = jnp.where(s < NZ * NX * NC - 1, 1.0, 0.0).astype(F32)
 
-    def project(col, rows):
-        w = win[:, :, :, :, col : col + 256].reshape(D, 256)
+    def project(weights, col, rows):
+        w = weights[:, :, :, :, col : col + 256].reshape(D, 256)
         return jnp.dot(nrm[:rows, :], w, preferred_element_type=F32).astype(BF16)
 
     for n in range(2):
-        u = project(CH + n * 256, TOK + 2 * PAD)
+        u = project(wl, n * 256, TOK + 2 * PAD)
         for k in range(2):
             v = u[:, k * 128 : (k + 1) * 128].astype(F32)
             ulf[2 * n + k, PAD : PAD + TOK, :] = v[:TOK]
             ulf[2 * n + k, 0:PAD, :] = v[TOK : TOK + PAD] * has_before
             ulf[2 * n + k, PAD + TOK :, :] = v[TOK + PAD :] * has_after
-    serve(out_b[3], out_a[2])
-    serve(out_rows[0])
+    serve(out_b[1], out_x[1], out_a[1])
     for load in loads[4:6]:
         load.wait()
 
@@ -363,6 +365,7 @@
     block(0)
     block(1)
     block(2)
+    serve(pool_a[5], pool_rows[3], pool_rows[4])
     block(3)
 
     def scan_step(t, carry):
@@ -400,13 +403,14 @@
     for dx, dc in around:
         links.put(c1.at[me], c1.at[me], g_k1, k1, sp_1=xx(dx), sp_2=lax.rem(c + dc, NC))
 
+    serve(out_b[2], out_a[2])
+    pool_arrived(0)
     for n in range(2):
-        pext[OWN : OWN + TOK, n * 256 : (n + 1) * 256] = project(n * 256, TOK)
+        pext[OWN : OWN + TOK, n * 256 : (n + 1) * 256] = project(wp, n * 256, TOK)
     g_ph = links.group(pext.at[pl.ds(0, 2 * OWN)])
     ph = {d: links.slot() for d in (1, -1)}
     links.put(pext.at[pl.ds(TOK, OWN)], pext.at[pl.ds(0, OWN)], g_ph, ph[1], **after)
     links.put(pext.at[pl.ds(OWN, OWN)], pext.at[pl.ds(OWN + TOK, OWN)], g_ph, ph[-1], **before)
-    serve(out_b[4], out_a[3])
 
     def combine(table, mine):
         full, inside = [], []
@@ -432,6 +436,7 @@
         scale = jnp.concatenate([rcp[...], rcp[...]], axis=1)
         pdf[:, cols] = (total * scale - own).astype(BF16)
 
+    serve(out_x[2])
     links.got(c1.at[pl.ds(0, 7)], k1, **after)
     full, near = combine(c1, me)
     for d in range(2):
@@ -441,7 +446,7 @@
     for d in range(1, NZ):
         links.put(c2.at[z], c2.at[z], g_k2, k2, sp_0=zz(d))
 
-    serve(out_rows[1], out_rows[2], out_a[4])
+    serve(out_b[3], out_x[3], out_a[3], out_rows[0], out_rows[1])
     loads[3].wait()
     links.got(pext.at[pl.ds(0, OWN)], ph[1], **after)
     links.got(pext.at[pl.ds(OWN + TOK, OWN)], ph[-1], **before)
@@ -451,7 +456,6 @@
         cols = slice(n * 256, (n + 1) * 256)
         ycat[:, cols] = jnp.dot(pdf[...], pmv[0, :, cols], preferred_element_type=F32).astype(BF16)
 
-    serve(out_rows[3])
     links.got(c2.at[pl.ds(0, 7)], k2, **after)
     _, far = combine(c2, z)
     for d in range(2):
@@ -494,7 +498,9 @@
         links.put(part.at[yy(2), :, here], rs2.at[:, here], g_q2, q2[n], tp=yy(d))
         links.put(part.at[yy(-d), :, here], rs1.at[:, tile(n)], g_q1, q1, tp=yy(-d))
         pltpu.make_async_copy(part.at[y, :, here], own.at[:, tile(n)], local.at[0]).start()
-        if n == 2:
+        if n == 1:
+            serve(out_b[4], out_x[4], out_a[4], out_rows[2], out_rows[3])
+        if n == 4:
             serve(out_a[5], out_rows[4])
         if n >= 5:
             relay(n - 5)
@@ -524,7 +530,8 @@
         scratch_shapes=[
             buf((NY, TOK, CH), BF16),
             buf((TOK + 2 * PAD, D), BF16),
-            buf((NZ, NX, NC, 32, 2 * CH), BF16),
+            buf((NZ, NX, NC, 32, CH), BF16),
+            buf((NZ, NX, NC, 32, CH), BF16),
             buf((NZ, NX, NC, 32, 2 * CH), BF16),
             buf((1, CH, CH), BF16),
             buf((2, 4, 128, 128), BF16),

time: 68.3 us -> 67.2 us (0.984)
  Pallas kernels: 66 us -> 64.6 us
    pallas_call x1, Pallas kernels: 66 us -> 64.6 us  [per_device(): pl.pallas_call(layer, out_shape=[jax.ShapeDtypeStruct((OUT_ROWS, D), BF16...]
where the time goes in v8:
time: 67.2 us; the launch traced here: 66.7 us
  Pallas kernels  64.6 us (96%)
  other arithmetic  2.13 us (3%)
    pallas_call x1, Pallas kernels, per_device(): pl.pallas_call(layer, out_shape=[jax.ShapeDtypeStruct((OUT_ROWS, D), BF16...  64.6 us
    convert_element_type x1, other arithmetic, per_device(): return total.astype(BF16)  2.13 us

profile of v8, /device:TPU:8, one launch (start us, length us, event | category | flops | bytes accessed | tf_op | source)
XLA Modules:
  0.0 66.7 jit_solution(16310387124293947229)
XLA Ops:
  0.0 64.6 %layer.1 = (bf16[96,2048]{1,0:T(8,128)(2,1)}, bf16[96,2048]{1,0:T(8,128)(2,1)}, bf16[96,2048]{1,0:T(8,128)(2,1)}) custom-call(bf16[384,512]{1,0:T(8,128)(2,1)} %tokens.1, f32[1,2048]{1,0:T(1,128)} %bitcast.5, bf16[32,512]{1,0:T(8,128)(2,1)} %wpi.1, bf16[32,512]{1,0:T(8,128)(2,1)} %wli.1, bf16[1,512,512]{2,1,0:T(8,128)(2,1)} %pmix.1, bf16[4,512]{1,0:T(4,128)(2,1)} %taps.1, ...), custom_call_target="tpu_custom_call" | custom-call | tf_op jit(solution)/shard_map/layer/pallas_call | solution.py:522
  64.6 2.1 %add_convert_fusion = bf16[96,2048]{1,0:T(8,128)(2,1)} fusion(bf16[96,2048]{1,0:T(8,128)(2,1)} %get-tuple-element.10, bf16[96,2048]{1,0:T(8,128)(2,1)} %get-tuple-element.9, bf16[96,2048]{1,0:T(8,128)(2,1)} %get-tuple-element.8), kind=kLoop, calls=%fused_computation | loop fusion | flops 1179648 | bytes 1572864 | tf_op jit(solution)/shard_map/convert_element_type | solution.py:571

commit v9 on v8

--- a/solution.py
+++ b/solution.py
@@ -25,7 +25,7 @@
 PAD = 16
 OUT_ROWS = TOK // NY
 N_SEND = 25
-N_RECV = 171
+N_RECV = 148
 N_LOCAL = 8
 F32 = jnp.float32
 BF16 = jnp.bfloat16
@@ -78,12 +78,16 @@
     both = (1, -1)
     rel = [0, -1, 1, -2, 2, -3, 3, 4]
     a1 = {dx: links.slot() for dx in (1, 3, 2)}
+    turn_slots = [links.slot() for _ in range(5)] if by_row else []
     a2 = {
-        (s, k, e): links.slot()
+        (s, k, e): 0 if by_row else links.slot()
         for s in both
         for e in range(NX)
         for k in range(1, 5 if (s == 1) == (e < 2) else 4)
     }
+    turns = [[p for p in a2 if p[1] + (p[2] > 0) == r] for r in range(6)]
+    if by_row:
+        a2 = {p: slot for turn, slot in zip(turns[1:], turn_slots) for p in turn}
     b1 = {(s, k): links.slot() for s in both for k in range(1, 5 if s == 1 else 4)}
     b2 = {d: links.slot() for d in rel}
     dd = {d: links.slot() for d in rel} if by_row else dict.fromkeys(rel, links.slot())
@@ -103,6 +107,11 @@
             links.got(buf.at[zz(-s * k), xx(e), c, lo], a2[s, k, e], sp_0=zz(s))
             a_send(s, k + 1, e)
 
+    def a_turn(r):
+        links.got(buf.at[pl.ds(0, len(turns[r])), 0, c, lo], turn_slots[r - 1], sp_0=zz(1))
+        for s, k, e in turns[r]:
+            a_send(s, k + 1, e)
+
     def a_side(dx):
         links.got(buf.at[z, xx(-dx), c, lo], a1[dx], sp_1=xx(dx))
         for s in both:
@@ -153,6 +162,9 @@
             [at(a_hop, s, k, 0) for s in both]
             + [at(a_hop, s, k - 1, e) for e in (3, 1, 2) for s in both]
         )
+    if by_row:
+        along_a[1] = [at(a_side, 1), at(a_side, 3), at(a_turn, 1), at(a_side, 2)]
+        along_a[2:] = [[at(a_turn, r)] for r in range(2, 6)]
     rows = [[at(row_done, d) for d in ds] for ds in ((0,), (-1, 1), (-2, 2), (-3, 3), (4,))]
     spread = [[at(b_spread, d) for d in ds] for ds in ((0,), (-1, 1), (-2, 2), (-3, 3), (4,))]
     return along_a, along_b, rows, arrived, spread

time: 67.2 us -> 67.1 us (level)
  no operation moved by 1% of the time
where the time goes in v9:
time: 67.1 us; the launch traced here: 66.9 us
  Pallas kernels  64.8 us (97%)
  other arithmetic  2.13 us (3%)
    pallas_call x1, Pallas kernels, per_device(): pl.pallas_call(layer, out_shape=[jax.ShapeDtypeStruct((OUT_ROWS, D), BF16...  64.8 us
    convert_element_type x1, other arithmetic, per_device(): return total.astype(BF16)  2.13 us

profile of v9, /device:TPU:8, one launch (start us, length us, event | category | flops | bytes accessed | tf_op | source)
XLA Modules:
  0.0 66.9 jit_solution(10013236241588007284)
XLA Ops:
  0.0 64.8 %layer.1 = (bf16[96,2048]{1,0:T(8,128)(2,1)}, bf16[96,2048]{1,0:T(8,128)(2,1)}, bf16[96,2048]{1,0:T(8,128)(2,1)}) custom-call(bf16[384,512]{1,0:T(8,128)(2,1)} %tokens.1, f32[1,2048]{1,0:T(1,128)} %bitcast.5, bf16[32,512]{1,0:T(8,128)(2,1)} %wpi.1, bf16[32,512]{1,0:T(8,128)(2,1)} %wli.1, bf16[1,512,512]{2,1,0:T(8,128)(2,1)} %pmix.1, bf16[4,512]{1,0:T(4,128)(2,1)} %taps.1, ...), custom_call_target="tpu_custom_call" | custom-call | tf_op jit(solution)/shard_map/layer/pallas_call | solution.py:534
  64.8 2.1 %add_convert_fusion = bf16[96,2048]{1,0:T(8,128)(2,1)} fusion(bf16[96,2048]{1,0:T(8,128)(2,1)} %get-tuple-element.10, bf16[96,2048]{1,0:T(8,128)(2,1)} %get-tuple-element.9, bf16[96,2048]{1,0:T(8,128)(2,1)} %get-tuple-element.8), kind=kLoop, calls=%fused_computation | loop fusion | flops 1179648 | bytes 1572864 | tf_op jit(solution)/shard_map/convert_element_type | solution.py:583
